TPU v7x, 32 devices: a whole 2x2x4 slice. The times are simulated.
32 devices in a mesh: sp: 8 (over z, y), tp: 4 (over x, core).
Axes of the slice: x: 2, y: 2, z: 4, core: 2. Of those that a mesh axis runs over, the one named last changes fastest.
Arguments:
- inputs: bfloat16 [4096, 4096], P('sp', 'tp'), may hold values from -24 to 24
- length: int32 [1], replicated, may hold values from 2049 to 4096
- win_query: bfloat16 [4096, 1536], P(None, 'tp'), may hold values from -8 to 8
- win_key: bfloat16 [4096, 512], P(None, 'tp'), may hold values from -8 to 8
- win_value: bfloat16 [4096, 512], P(None, 'tp'), may hold values from -1.5 to 1.5
- sink_logit: float32 [24], P('tp'), may hold values from 4 to 8
- diff_query: bfloat16 [4096, 1024], P(None, 'tp'), may hold values from -8 to 8
- diff_key: bfloat16 [4096, 1024], P(None, 'tp'), may hold values from -8 to 8
- diff_value: bfloat16 [4096, 1024], P(None, 'tp'), may hold values from -0.09375 to 0.09375
- mix_lambda: float32 [16], P('tp'), may hold values from 0.3 to 0.8
- head_gain: float32 [64], replicated, may hold values from 0.1 to 1.9
- win_out: bfloat16 [1536, 4096], P('tp'), may hold values from -0.125 to 0.125
- diff_out: bfloat16 [1024, 4096], P('tp'), may hold values from -0.125 to 0.125
Outputs:
- merged_out: bfloat16 [4096, 4096], P(('sp', 'tp'))
All inputs are finite; a program needn't handle non-finite values.
Results may differ from a plain program's by a relative error of at most 0.015.
Values may be sent and summed in bfloat16 or wider, within the bound.
A program may use at most 128 MiB of HBM per device.

v0:
```python
import jax
import jax.numpy as jnp
from jax import lax
from jax.sharding import PartitionSpec as P

HEAD = 64
DQK = 32
GROUP = 3
WINDOW = 128


epsilon = 1e-06
masked_score = -1e30


def extended(block, sides, width):
    for axis, dim in sides:
        count = lax.axis_size(axis)
        forward = [(i, i + 1) for i in range(count - 1)]
        backward = [(target, source) for source, target in forward]
        low = lax.ppermute(
            lax.slice_in_dim(block, block.shape[dim] - width, None, axis=dim), axis, forward
        )
        high = lax.ppermute(lax.slice_in_dim(block, 0, width, axis=dim), axis, backward)
        block = jnp.concatenate([low, block, high], axis=dim)
    return block


def window_part(win_q, win_k, win_v, sink_logit, live_count, offset):
    row_count = win_q.shape[0]
    kv_local = win_k.shape[1] // HEAD
    stacked = jnp.stack(
        (win_k.reshape(row_count, kv_local, HEAD), win_v.reshape(row_count, kv_local, HEAD)), axis=2
    )
    stacked = stacked.reshape(row_count, kv_local * 2 * HEAD)
    padded = extended(stacked, (("sp", 0),), WINDOW)
    padded = padded.reshape(row_count + 2 * WINDOW, kv_local, 2, HEAD)
    keys_win = padded[:, :, 0]
    values_win = padded[:, :, 1]
    queries = win_q.reshape(row_count, kv_local, GROUP, HEAD)
    sink_table = sink_logit.reshape(kv_local, GROUP)
    query_pos = offset + jnp.arange(row_count, dtype=jnp.int32)
    key_pos = offset - WINDOW + jnp.arange(row_count + 2 * WINDOW, dtype=jnp.int32)
    allowed = (
        (jnp.abs(query_pos[:, None] - key_pos[None, :]) <= WINDOW)
        & (key_pos[None, :] >= 0)
        & (key_pos[None, :] < live_count)
    )
    scores = jnp.einsum(
        "qhgd,khd->hgqk", queries, keys_win, preferred_element_type=jnp.float32
    ) * HEAD ** (-0.5)
    scores = jnp.where(allowed[None, None], scores, masked_score)
    row_max = jnp.maximum(jnp.max(scores, axis=-1), sink_table[:, :, None])
    exponent = jnp.where(allowed[None, None], jnp.exp(scores - row_max[..., None]), 0.0)
    denominator = jnp.sum(exponent, axis=-1) + jnp.exp(sink_table[:, :, None] - row_max)
    result = jnp.einsum(
        "hgqk,khd->qhgd",
        exponent.astype(jnp.bfloat16),
        values_win,
        preferred_element_type=jnp.float32,
    )
    result = result / jnp.transpose(denominator, (2, 0, 1))[..., None]
    result = jnp.where((query_pos < live_count)[:, None, None, None], result, 0.0)
    return result.reshape(row_count, kv_local * GROUP * HEAD).astype(jnp.bfloat16)


def attend(running, queries, key_part, value_part, live_count, block_total, query_step):
    key_length = key_part.shape[0]
    key_step = 4096

    def one_query_block(block_index, block_state):
        running_max, total_sum, weighted = block_state
        row_begin = block_index * query_step
        query_slab = lax.dynamic_slice_in_dim(queries, row_begin, query_step, 0)
        start_state = (
            lax.dynamic_slice_in_dim(running_max, row_begin, query_step, 2),
            lax.dynamic_slice_in_dim(total_sum, row_begin, query_step, 2),
            lax.dynamic_slice_in_dim(weighted, row_begin, query_step, 2),
        )

        def one_key_block(key_index, key_state):
            block_max, block_sum, block_weighted = key_state
            key_begin = key_index * key_step
            key_slab = lax.dynamic_slice_in_dim(key_part, key_begin, key_step, 0)
            value_slab = lax.dynamic_slice_in_dim(value_part, key_begin, key_step, 0)
            key_pos = key_begin + jnp.arange(key_step, dtype=jnp.int32)
            allowed = key_pos < live_count
            scores = jnp.einsum(
                "qhmd,khmd->hmqk", query_slab, key_slab, preferred_element_type=jnp.float32
            ) * DQK ** (-0.5)
            scores = jnp.where(allowed, scores, masked_score)
            new_max = jnp.maximum(block_max, jnp.max(scores, axis=-1))
            rescale = jnp.exp(block_max - new_max)
            exponent = jnp.where(allowed, jnp.exp(scores - new_max[..., None]), 0.0)
            new_total = block_sum * rescale + jnp.sum(exponent, axis=-1)
            new_weighted = block_weighted * rescale[..., None] + jnp.einsum(
                "hmqk,khd->hmqd",
                exponent.astype(jnp.bfloat16),
                value_slab,
                preferred_element_type=jnp.float32,
            )
            return (new_max, new_total, new_weighted)

        final_state = lax.fori_loop(0, key_length // key_step, one_key_block, start_state)
        return (
            lax.dynamic_update_slice_in_dim(running_max, final_state[0], row_begin, 2),
            lax.dynamic_update_slice_in_dim(total_sum, final_state[1], row_begin, 2),
            lax.dynamic_update_slice_in_dim(weighted, final_state[2], row_begin, 2),
        )

    return lax.fori_loop(0, block_total, one_query_block, running)


def diff_part(diff_q, diff_k, diff_v, mix_lambda, head_gain, live_count, offset):
    row_count = diff_q.shape[0]
    heads_local = mix_lambda.shape[0]
    query_step = 128
    positions = offset + jnp.arange(row_count, dtype=jnp.int32)
    live_rows = jnp.sum((positions < live_count).astype(jnp.int32))
    block_total = (live_rows + query_step - 1) // query_step
    queries = diff_q.reshape(row_count, heads_local, 2, DQK)
    zero_state = (
        jnp.full((heads_local, 2, row_count), masked_score, jnp.float32),
        jnp.zeros((heads_local, 2, row_count), jnp.float32),
        jnp.zeros((heads_local, 2, row_count, HEAD), jnp.float32),
    )
    key_part = lax.all_gather(diff_k, "sp", axis=0, tiled=True).reshape(-1, heads_local, 2, DQK)
    value_part = lax.all_gather(diff_v, "sp", axis=0, tiled=True).reshape(-1, heads_local, HEAD)
    running = lax.cond(
        jnp.int32(0) < live_count,
        lambda inner_state: attend(
            inner_state, queries, key_part, value_part, live_count, block_total, query_step
        ),
        lambda inner_state: inner_state,
        zero_state,
    )
    total_sum = running[1]
    safe_total = jnp.where(total_sum > 0.0, total_sum, 1.0)
    map_rows = running[2] / safe_total[..., None]
    mixed_rows = map_rows[:, 0] - mix_lambda[:, None, None] * map_rows[:, 1]
    normed = (
        mixed_rows
        * lax.rsqrt(jnp.mean(mixed_rows * mixed_rows, axis=-1, keepdims=True) + epsilon)
        * head_gain
    )
    normed = jnp.where((positions < live_count)[None, :, None], normed, 0.0)
    result = (
        jnp.transpose(normed, (1, 0, 2)).reshape(row_count, heads_local * HEAD).astype(jnp.bfloat16)
    )
    return result


def body(
    inputs,
    length,
    win_query,
    win_key,
    win_value,
    sink_logit,
    diff_query,
    diff_key,
    diff_value,
    mix_lambda,
    head_gain,
    win_out,
    diff_out,
):
    row_count = inputs.shape[0]
    live_count = length[0]
    weights = (win_query, win_key, win_value, diff_query, diff_key, diff_value)
    segment = lax.all_gather(inputs, "tp", axis=1, tiled=True)
    summed = tuple(
        (jnp.dot(segment, weight, preferred_element_type=jnp.float32) for weight in weights)
    )
    win_q, win_k, win_v, diff_q, diff_k, diff_v = [total.astype(jnp.bfloat16) for total in summed]
    offset = lax.axis_index("sp") * row_count
    win_rows = window_part(win_q, win_k, win_v, sink_logit, live_count, offset)
    diff_rows = diff_part(diff_q, diff_k, diff_v, mix_lambda, head_gain, live_count, offset)
    partial_value = jnp.dot(win_rows, win_out, preferred_element_type=jnp.float32)
    return lax.psum_scatter(
        (partial_value + jnp.dot(diff_rows, diff_out, preferred_element_type=jnp.float32)).astype(
            jnp.bfloat16
        ),
        "tp",
        scatter_dimension=0,
        tiled=True,
    )


def solution(mesh):
    placed = (
        P("sp", "tp"),
        P(),
        P(None, "tp"),
        P(None, "tp"),
        P(None, "tp"),
        P("tp"),
        P(None, "tp"),
        P(None, "tp"),
        P(None, "tp"),
        P("tp"),
        P(),
        P("tp", None),
        P("tp", None),
    )
    return jax.shard_map(
        body, mesh=mesh, in_specs=placed, out_specs=P(("sp", "tp"), None), check_vma=False
    )
```

profile of v0, /device:TPU:0, one launch (start us, length us, event | category | flops | bytes accessed | tf_op | source)
XLA Modules:
  0.0 299.4 jit_solution(1611999572940378291)
XLA Ops:
  7.3 38.8 %all-gather.4.cloned.1.call-done = bf16[512,4096]{1,0:T(8,128)(2,1)} async-done(((bf16[512,1024]{1,0:T(8,128)(2,1)}), bf16[512,4096]{1,0:T(8,128)(2,1)}) %all-gather.4.cloned.1.call-update) | async-done | bytes 4194320 | tf_op jit(solution)/shard_map/all_gather | solution.py:171
  46.1 4.8 %convolution_convert_fusion.1 = bf16[512,256]{1,0:T(8,128)(2,1)} fusion(bf16[512,4096]{1,0:T(8,128)(2,1)} %all-gather.4.cloned.1.call-done, bf16[4096,256]{1,0:T(8,128)(2,1)} %param.25), kind=kOutput, calls=%fused_computation.34 | convolution fusion | flops 1073872896 | bytes 6553600 | tf_op jit(solution)/shard_map/dot_general | solution.py:173
  52.6 4.4 %convolution_convert_fusion.4 = bf16[512,128]{0,1:T(8,128)(2,1)S(1)} fusion(bf16[512,4096]{1,0:T(8,128)(2,1)} %all-gather.4.cloned.1.call-done, bf16[4096,128]{1,0:T(8,128)(2,1)} %param.21), kind=kOutput, calls=%fused_computation.37 | convolution fusion | flops 536936448 | bytes 5373952 | tf_op jit(solution)/shard_map/dot_general | solution.py:173
  57.0 1.5 convolution_convert_fusion.5
  61.8 5.2 %collective-permute-start = (bf16[128,256]{0,1:T(8,128)(2,1)}, bf16[128,256]{0,1:T(8,128)(2,1)}, u32[]{:S(2)}, u32[]{:S(2)}) collective-permute-start(bf16[128,256]{0,1:T(8,128)(2,1)} %bitcast.8), channel_id=1, source_target_pairs={{0,4},{4,8},{8,12},{12,16},{16,20},{20,24},{24,28},{1,5},{5,9},{9,... | collective-permute-start | bytes 196616 | tf_op jit(solution)/shard_map/ppermute | solution.py:21
  67.0 2.0 convolution_convert_fusion.2
  69.2 5.2 %convolution_convert_fusion = bf16[512,384]{0,1:T(8,128)(2,1)S(1)} fusion(bf16[512,4096]{1,0:T(8,128)(2,1)} %all-gather.4.cloned.1.call-done, bf16[4096,384]{1,0:T(8,128)(2,1)} %param.19), kind=kOutput, calls=%fused_computation.33 | convolution fusion | flops 1610809344 | bytes 7733248 | tf_op jit(solution)/shard_map/dot_general | solution.py:173
  74.4 2.0 convolution_convert_fusion.3
  77.3 1.7 fusion.23
  79.1 2.3 fusion.24
  81.4 2.7 fusion.40
  84.1 5.6 %fusion.52 = f32[512,4096]{1,0:T(8,128)} fusion(bf16[512,384]{0,1:T(8,128)(2,1)S(1)} %bitcast.123, bf16[384,4096]{1,0:T(8,128)(2,1)S(1)} %copy-done), kind=kOutput, calls=%fused_computation.68 | convolution fusion | flops 1610612736 | bytes 11927552 | tf_op jit(solution)/shard_map/dot_general | solution.py:179
  89.7 11.3 %all-gather.8.cloned.1.call-done = bf16[4096,256]{1,0:T(8,128)(2,1)} async-done(((bf16[512,256]{1,0:T(8,128)(2,1)}), bf16[4096,256]{1,0:T(8,128)(2,1)}) %all-gather.8.cloned.1.call-update) | async-done | bytes 2097168 | tf_op jit(solution)/shard_map/all_gather | solution.py:128
  101.0 49.8 %all-gather.6.cloned.1.call-done = bf16[4096,256]{1,0:T(8,128)(2,1)} async-done(((bf16[512,256]{1,0:T(8,128)(2,1)}), bf16[4096,256]{1,0:T(8,128)(2,1)}) %all-gather.6.cloned.1.call-update) | async-done | bytes 2097168 | tf_op jit(solution)/shard_map/all_gather | solution.py:127
  150.8 89.2 %conditional.1 = (f32[4,2,512]{2,1,0:T(2,128)}, f32[4,2,512,64]{2,3,1,0:T(8,128)}) conditional(s32[]{:T(128)} %convert_element_type.55, () %tuple.34, (s32[512]{0:T(512)S(1)}, bf16[512,256]{1,0:T(8,128)(2,1)S(1)}, bf16[4096,256]{1,0:T(8,128)(2,1)}, bf16[4096,256]{1,0:T(8,128)(2,1)}, s32[]{:T(128)}, /*index=5*/s32[]{:T(128)}) %tuple.79), branch_computations={%region_3.4_spmd, %region_4.9_spmd.clone} | conditional | flops 859970048 | bytes 132364824 | solution.py:129
  152.3 4.1 %copy.34 = bf16[4096,256]{0,1:T(8,128)(2,1)} copy(bf16[4096,256]{1,0:T(8,128)(2,1)} %get-tuple-element.250) | data formatting | bytes 4194304 | tf_op jit(solution)/shard_map
  156.4 2.9 copy.33
  161.0 79.0 %while.37 = (s32[]{:T(128)}, f32[4,2,512]{2,1,0:T(2,128)S(1)}, f32[4,2,512]{2,1,0:T(2,128)}, f32[4,2,512,64]{2,3,1,0:T(8,128)}, s32[]{:T(128)}, /*index=5*/s32[]...) while((s32[]{:T(128)}, f32[4,2,512]{2,1,0:T(2,128)S(1)}, ...), condition=%wide.region_8.8_spmd, body=%wide.region_5.7_spmd.sunk | while | flops 859969536 | bytes 122368224 | solution.py:111
  161.7 2.7 fusion.82
  164.5 4.9 %fusion.83 = f32[4,2,128]{2,1,0:T(2,128)S(1)} fusion(f32[4,2,128,4096]{3,2,1,0:T(8,128)S(1)} %get-tuple-element.357, f32[4,2,128]{2,1,0:T(2,128)S(1)} %get-tuple-element.358, pred[4096]{0:T(1024)(128)(4,1)S(1)} %iota_compare_fusion.2), kind=kLoop, calls=%fused_computation.4.clone.1 | loop fusion | flops 20970496 | bytes 16789504 | tf_op jit(solution)/shard_map/cond/branch_1_fun/while/body/while/body/eval_jaxpr/reduce_sum | solution.py:95
  171.5 9.3 %fusion.84 = f32[4,2,512,64]{2,3,1,0:T(8,128)} fusion(f32[4,2,512,64]{2,3,1,0:T(8,128)} %get-tuple-element.377, s32[]{:T(128)S(6)} %select_n.128, bf16[4096,4,64]{0,2,1:T(8,128)(2,1)} %get-tuple-element.395, f32[4,2,128,4096]{3,2,1,0:T(8,128)} %copy-done.2, f32[4,2,128]{2,1,0:T(2,128)S(1)} %get-tuple-element.358, ...), kind=kOutput, calls=%fused_computation.9.clone.1 | convolution fusion | flops 557973504 | bytes 19410948 | tf_op jit(solution)/shard_map/cond/branch_1_fun/while/body/while/body/eval_jaxpr/hmqk,khd->hmqd/dot_general | solution.py:96
  181.5 2.7 fusion.82
  184.2 4.9 %fusion.83 = f32[4,2,128]{2,1,0:T(2,128)S(1)} fusion(f32[4,2,128,4096]{3,2,1,0:T(8,128)S(1)} %get-tuple-element.357, f32[4,2,128]{2,1,0:T(2,128)S(1)} %get-tuple-element.358, pred[4096]{0:T(1024)(128)(4,1)S(1)} %iota_compare_fusion.2), kind=kLoop, calls=%fused_computation.4.clone.1 | loop fusion | flops 20970496 | bytes 16789504 | tf_op jit(solution)/shard_map/cond/branch_1_fun/while/body/while/body/eval_jaxpr/reduce_sum | solution.py:95
  191.2 9.3 %fusion.84 = f32[4,2,512,64]{2,3,1,0:T(8,128)} fusion(f32[4,2,512,64]{2,3,1,0:T(8,128)} %get-tuple-element.377, s32[]{:T(128)S(6)} %select_n.128, bf16[4096,4,64]{0,2,1:T(8,128)(2,1)} %get-tuple-element.395, f32[4,2,128,4096]{3,2,1,0:T(8,128)} %copy-done.2, f32[4,2,128]{2,1,0:T(2,128)S(1)} %get-tuple-element.358, ...), kind=kOutput, calls=%fused_computation.9.clone.1 | convolution fusion | flops 557973504 | bytes 19410948 | tf_op jit(solution)/shard_map/cond/branch_1_fun/while/body/while/body/eval_jaxpr/hmqk,khd->hmqd/dot_general | solution.py:96
  201.2 2.7 fusion.82
  204.0 4.9 %fusion.83 = f32[4,2,128]{2,1,0:T(2,128)S(1)} fusion(f32[4,2,128,4096]{3,2,1,0:T(8,128)S(1)} %get-tuple-element.357, f32[4,2,128]{2,1,0:T(2,128)S(1)} %get-tuple-element.358, pred[4096]{0:T(1024)(128)(4,1)S(1)} %iota_compare_fusion.2), kind=kLoop, calls=%fused_computation.4.clone.1 | loop fusion | flops 20970496 | bytes 16789504 | tf_op jit(solution)/shard_map/cond/branch_1_fun/while/body/while/body/eval_jaxpr/reduce_sum | solution.py:95
  211.0 9.3 %fusion.84 = f32[4,2,512,64]{2,3,1,0:T(8,128)} fusion(f32[4,2,512,64]{2,3,1,0:T(8,128)} %get-tuple-element.377, s32[]{:T(128)S(6)} %select_n.128, bf16[4096,4,64]{0,2,1:T(8,128)(2,1)} %get-tuple-element.395, f32[4,2,128,4096]{3,2,1,0:T(8,128)} %copy-done.2, f32[4,2,128]{2,1,0:T(2,128)S(1)} %get-tuple-element.358, ...), kind=kOutput, calls=%fused_computation.9.clone.1 | convolution fusion | flops 557973504 | bytes 19410948 | tf_op jit(solution)/shard_map/cond/branch_1_fun/while/body/while/body/eval_jaxpr/hmqk,khd->hmqd/dot_general | solution.py:96
  221.0 2.7 fusion.82
  223.7 4.9 %fusion.83 = f32[4,2,128]{2,1,0:T(2,128)S(1)} fusion(f32[4,2,128,4096]{3,2,1,0:T(8,128)S(1)} %get-tuple-element.357, f32[4,2,128]{2,1,0:T(2,128)S(1)} %get-tuple-element.358, pred[4096]{0:T(1024)(128)(4,1)S(1)} %iota_compare_fusion.2), kind=kLoop, calls=%fused_computation.4.clone.1 | loop fusion | flops 20970496 | bytes 16789504 | tf_op jit(solution)/shard_map/cond/branch_1_fun/while/body/while/body/eval_jaxpr/reduce_sum | solution.py:95
  230.7 9.3 %fusion.84 = f32[4,2,512,64]{2,3,1,0:T(8,128)} fusion(f32[4,2,512,64]{2,3,1,0:T(8,128)} %get-tuple-element.377, s32[]{:T(128)S(6)} %select_n.128, bf16[4096,4,64]{0,2,1:T(8,128)(2,1)} %get-tuple-element.395, f32[4,2,128,4096]{3,2,1,0:T(8,128)} %copy-done.2, f32[4,2,128]{2,1,0:T(2,128)S(1)} %get-tuple-element.358, ...), kind=kOutput, calls=%fused_computation.9.clone.1 | convolution fusion | flops 557973504 | bytes 19410948 | tf_op jit(solution)/shard_map/cond/branch_1_fun/while/body/while/body/eval_jaxpr/hmqk,khd->hmqd/dot_general | solution.py:96
  242.7 6.8 %add_convert_fusion = bf16[512,4096]{1,0:T(8,128)(2,1)} fusion(f32[512,4096]{1,0:T(8,128)} %fusion.52, bf16[512,256]{0,1:T(8,128)(2,1)S(1)} %bitcast.122, bf16[256,4096]{1,0:T(8,128)(2,1)S(1)} %copy-done.5), kind=kOutput, calls=%fused_computation.23 | convolution fusion | flops 1077936128 | bytes 14942208 | tf_op jit(solution)/shard_map/dot_general | solution.py:181
  249.6 43.3 %reduce-scatter.2.cloned.1.call-done = bf16[128,4096]{1,0:T(8,128)(2,1)} async-done(((bf16[512,4096]{1,0:T(8,128)(2,1)}), bf16[128,4096]{1,0:T(8,128)(2,1)}) %reduce-scatter.2.cloned.1.call-update) | async-done | bytes 1048592 | tf_op jit(solution)/shard_map/reduce_scatter | solution.py:180
  (93 shorter events, 22.6 us)
Async XLA Ops:
  6.5 77.6 %copy-start = (bf16[384,4096]{1,0:T(8,128)(2,1)S(1)}, bf16[384,4096]{1,0:T(8,128)(2,1)}, u32[]{:S(2)}) copy-start(bf16[384,4096]{1,0:T(8,128)(2,1)} %param.28) | copy-start | bytes 9437188
  6.5 39.6 %all-gather.4.cloned.1.call-start = ((), (), s32[]{:S(2)}) async-start(), calls=%async_computation.1 | async-start | bytes 5242880 | tf_op jit(solution)/shard_map/all_gather | solution.py:171
  7.3 44.4 %copy-start.16 = (f32[6]{0:T(128)S(1)}, f32[6]{0:T(128)}, u32[]{:S(2)}) copy-start(f32[6]{0:T(128)} %param.22) | copy-start | bytes 76
  7.3 93.7 %all-gather.8.cloned.1.call-start = ((), (), s32[]{:S(2)}) async-start(), calls=%async_computation.3 | async-start | bytes 2359296 | tf_op jit(solution)/shard_map/all_gather | solution.py:128
  51.0 99.8 %all-gather.6.cloned.1.call-start = ((), (), s32[]{:S(2)}) async-start(), calls=%async_computation.2 | async-start | bytes 2359296 | tf_op jit(solution)/shard_map/all_gather | solution.py:127
  51.8 5.2 %copy-start.3 = (bf16[512,4096]{1,0:T(8,128)(2,1)S(1)}, bf16[512,4096]{1,0:T(8,128)(2,1)}, u32[]{:S(2)}) copy-start(bf16[512,4096]{1,0:T(8,128)(2,1)} %all-gather.4.cloned.1.call-done) | copy-start | bytes 12582916
  51.8 5.2 %copy-start.10 = (bf16[4096,128]{1,0:T(8,128)(2,1)S(1)}, bf16[4096,128]{1,0:T(8,128)(2,1)}, u32[]{:S(2)}) copy-start(bf16[4096,128]{1,0:T(8,128)(2,1)} %param.20) | copy-start | bytes 3145732
  57.0 1.5 copy-start.6
  57.0 9.9 %copy-start.14 = (bf16[4096,256]{1,0:T(8,128)(2,1)S(1)}, bf16[4096,256]{1,0:T(8,128)(2,1)}, u32[]{:S(2)}) copy-start(bf16[4096,256]{1,0:T(8,128)(2,1)} %param.24) | copy-start | bytes 6291460
  58.6 0.7 copy-start.8
  60.5 15.9 %collective-permute-start.1 = (bf16[128,256]{0,1:T(8,128)(2,1)}, bf16[128,256]{0,1:T(8,128)(2,1)}, u32[]{:S(2)}, u32[]{:S(2)}) collective-permute-start(bf16[128,256]{0,1:T(8,128)(2,1)} %bitcast.10), channel_id=1, source_target_pairs={{4,0},{8,4},{12,8},{16,12},{20,16},{24,20},{28,24},{5,1},{9,5},{13... | collective-permute-start | bytes 196616 | tf_op jit(solution)/shard_map/ppermute | solution.py:24
  61.8 14.6 %collective-permute-start = (bf16[128,256]{0,1:T(8,128)(2,1)}, bf16[128,256]{0,1:T(8,128)(2,1)}, u32[]{:S(2)}, u32[]{:S(2)}) collective-permute-start(bf16[128,256]{0,1:T(8,128)(2,1)} %bitcast.8), channel_id=1, source_target_pairs={{0,4},{4,8},{8,12},{12,16},{16,20},{20,24},{24,28},{1,5},{5,9},{9,... | collective-permute-start | bytes 196616 | tf_op jit(solution)/shard_map/ppermute | solution.py:21
  69.0 223.9 %reduce-scatter.2.cloned.1.call-start = ((), (), s32[]{:S(2)}) async-start(), calls=%async_computation.4 | async-start | bytes 5242880 | tf_op jit(solution)/shard_map/reduce_scatter | solution.py:180
  69.2 5.2 %copy-start.4 = (bf16[512,4096]{1,0:T(8,128)(2,1)S(1)}, bf16[512,4096]{1,0:T(8,128)(2,1)}, u32[]{:S(2)}) copy-start(bf16[512,4096]{1,0:T(8,128)(2,1)} %all-gather.4.cloned.1.call-done) | copy-start | bytes 12582916
  69.2 5.2 %copy-start.15 = (bf16[4096,256]{1,0:T(8,128)(2,1)S(1)}, bf16[4096,256]{1,0:T(8,128)(2,1)}, u32[]{:S(2)}) copy-start(bf16[4096,256]{1,0:T(8,128)(2,1)} %param.23) | copy-start | bytes 6291460
  74.4 2.0 copy-start.7
  74.4 2.0 copy-start.9
  84.1 66.7 %copy-start.11 = (bf16[512,256]{1,0:T(8,128)(2,1)S(1)}, bf16[512,256]{1,0:T(8,128)(2,1)}, u32[]{:S(2)}) copy-start(bf16[512,256]{1,0:T(8,128)(2,1)} %convolution_convert_fusion.3) | copy-start | bytes 786436
  150.8 91.5 %copy-start.12 = (f32[4]{0:T(128)S(1)}, f32[4]{0:T(128)}, u32[]{:S(2)}) copy-start(f32[4]{0:T(128)} %param.26) | copy-start | bytes 52
  150.8 91.7 %copy-start.13 = (f32[64]{0:T(128)S(1)}, f32[64]{0:T(128)}, u32[]{:S(2)}) copy-start(f32[64]{0:T(128)} %param.27) | copy-start | bytes 772
  164.4 5.7 %copy-start.2 = (f32[4,2,128,4096]{3,2,1,0:T(8,128)}, f32[4,2,128,4096]{3,2,1,0:T(8,128)S(1)}, u32[]{:S(2)}) copy-start(f32[4,2,128,4096]{3,2,1,0:T(8,128)S(1)} %get-tuple-element.357) | copy-start | bytes 50331652 | tf_op jit(solution)/shard_map/cond/branch_1_fun/while
  184.2 5.7 %copy-start.2 = (f32[4,2,128,4096]{3,2,1,0:T(8,128)}, f32[4,2,128,4096]{3,2,1,0:T(8,128)S(1)}, u32[]{:S(2)}) copy-start(f32[4,2,128,4096]{3,2,1,0:T(8,128)S(1)} %get-tuple-element.357) | copy-start | bytes 50331652 | tf_op jit(solution)/shard_map/cond/branch_1_fun/while
  204.0 5.7 %copy-start.2 = (f32[4,2,128,4096]{3,2,1,0:T(8,128)}, f32[4,2,128,4096]{3,2,1,0:T(8,128)S(1)}, u32[]{:S(2)}) copy-start(f32[4,2,128,4096]{3,2,1,0:T(8,128)S(1)} %get-tuple-element.357) | copy-start | bytes 50331652 | tf_op jit(solution)/shard_map/cond/branch_1_fun/while
  223.7 5.7 %copy-start.2 = (f32[4,2,128,4096]{3,2,1,0:T(8,128)}, f32[4,2,128,4096]{3,2,1,0:T(8,128)S(1)}, u32[]{:S(2)}) copy-start(f32[4,2,128,4096]{3,2,1,0:T(8,128)S(1)} %get-tuple-element.357) | copy-start | bytes 50331652 | tf_op jit(solution)/shard_map/cond/branch_1_fun/while
  240.1 2.7 copy-start.5
  242.7 50.1 %copy-start.1 = (bf16[384,4096]{1,0:T(8,128)(2,1)S(1)}, bf16[384,4096]{1,0:T(8,128)(2,1)}, u32[]{:S(2)}) copy-start(bf16[384,4096]{1,0:T(8,128)(2,1)} %param.28) | copy-start | bytes 9437188
Sparse Core Ops, SparseCore 0:
  8.9 37.1 all-gather.3
  51.1 49.8 all-gather.7
  103.1 47.6 all-gather.5
  249.7 43.1 reduce-scatter.1
where the time goes:
time: 300 us; the launch traced here: 299 us
  waiting for transfers between devices  144 us (48%)
  matrix products  84.8 us (28%)
  other arithmetic  34.7 us (12%)
  local copies, waits for them, and re-layouts  14.3 us (5%)
  between operations  14.1 us (5%)
  starting transfers between devices  6.77 us (2%)
    all_gather x1, waiting for transfers between devices, diff_part(): lax.all_gather(diff_k, 'sp', axis=0, tiled=True)  49.8 us
    reduce_scatter x1, waiting for transfers between devices, body(): lax.psum_scatter((partial_value + jnp.dot(diff_rows, diff_out, preferred_...  43.3 us
    all_gather x1, waiting for transfers between devices, body(): segment = lax.all_gather(inputs, 'tp', axis=1, tiled=True)  38.8 us
    dot_general x4, matrix products, one_key_block(): jnp.einsum('hmqk,khd->hmqd', exponent.astype(jnp.bfloat16), value_slab, p...  37.3 us
    dot_general x6, matrix products, body(): jnp.dot(segment, weight, preferred_element_type=jnp.float32)  19.8 us
    reduce_sum x4, other arithmetic, one_key_block(): new_total = block_sum * rescale + jnp.sum(exponent, axis=-1)  19.5 us
    all_gather x1, waiting for transfers between devices, diff_part(): lax.all_gather(diff_v, 'sp', axis=0, tiled=True)  11.3 us
    dot_general x4, matrix products, one_key_block(): jnp.einsum('qhmd,khmd->hmqk', query_slab, key_slab, preferred_element_typ...  11 us
  transfers between devices with their start and end apart: 6, of which 4 were waited for; matrix products, arithmetic and copies ran while one was open for 10% of the time, Pallas kernels for 0%

commit v1 on v0

v1 whole, which is shorter than its diff:
```python
import functools

import jax
import jax.numpy as jnp
from jax import lax
from jax.experimental import pallas as pl
from jax.experimental.pallas import tpu as pltpu
from jax.sharding import PartitionSpec as P

HEAD = 64
DQK = 32
GROUP = 3
WINDOW = 128
LOG2E = 1.4426950408889634
NEG = -1e30
EPS = 1e-06
MESH = pl.DeviceIdType.MESH
VM = pl.BlockSpec(memory_space=pltpu.VMEM)
SM = pl.BlockSpec(memory_space=pltpu.SMEM)
F32 = jnp.float32
BF16 = jnp.bfloat16


def dot(a, b):
    return jnp.dot(a, b, preferred_element_type=F32)


def ring_to_sp(r, n):
    half = r // (n // 2)
    return (1 - half) * (2 * r) + half * (2 * (n - 1 - r) + 1)


def attention_kernel(
    n, length, sink, lam, gain, wqT, wk, wvT, dqT, dk, dvT,
    out, kbuf, vbuf, kwin, vwin, qz, acc, mx, ksem, vsem, hsem, lsem,
):
    rows = wk.shape[0]
    heads = dqT.shape[0] // HEAD
    kvh = wk.shape[1] // HEAD
    kw = min(2 * HEAD, wk.shape[1])
    sp = lax.axis_index("sp")
    y = sp % 2
    z = sp // 2
    me = z + y * (n - 1 - 2 * z)
    half = n // 2
    right = ring_to_sp((me + 1) % n, n)
    left = ring_to_sp((me + n - 1) % n, n)
    nxt = (sp + 1) % n
    prv = (sp + n - 1) % n
    barrier = pltpu.get_barrier_semaphore()
    for d in (left, right, prv, nxt):
        pl.semaphore_signal(barrier, inc=1, device_id={"sp": d}, device_id_type=MESH)
    pl.semaphore_wait(barrier, 4)

    W = WINDOW
    halos = []
    for i, (src, dst, to) in enumerate((
        (wk.at[pl.ds(rows - W, W)], kwin.at[pl.ds(0, W)], nxt),
        (wvT.at[:, pl.ds(rows - W, W)], vwin.at[:, pl.ds(0, W)], nxt),
        (wk.at[pl.ds(0, W)], kwin.at[pl.ds(rows + W, W)], prv),
        (wvT.at[:, pl.ds(0, W)], vwin.at[:, pl.ds(rows + W, W)], prv),
    )):
        c = pltpu.make_async_remote_copy(
            src_ref=src, dst_ref=dst, send_sem=hsem.at[0, i], recv_sem=hsem.at[1, i],
            device_id={"sp": to}, device_id_type=MESH)
        c.start()
        halos.append(c)

    def kcopy(direction, s, first=False):
        slot = (me + n - s) % n if direction == 0 else (me + s) % n
        return pltpu.make_async_remote_copy(
            src_ref=dk if first else kbuf.at[slot], dst_ref=kbuf.at[slot],
            send_sem=ksem.at[0, direction, s], recv_sem=ksem.at[1, direction, s],
            device_id={"sp": right if direction == 0 else left}, device_id_type=MESH)

    def vcopy(direction, s, first=False):
        slot = (me + n - s) % n if direction == 0 else (me + s) % n
        return pltpu.make_async_remote_copy(
            src_ref=dvT if first else vbuf.at[slot], dst_ref=vbuf.at[slot],
            send_sem=vsem.at[0, direction, s], recv_sem=vsem.at[1, direction, s],
            device_id={"sp": right if direction == 0 else left}, device_id_type=MESH)

    for d in (0, 1):
        kcopy(d, 0, True).start()
        vcopy(d, 0, True).start()

    local = [
        pltpu.make_async_copy(wk, kwin.at[pl.ds(W, rows)], lsem.at[0]),
        pltpu.make_async_copy(wvT, vwin.at[:, pl.ds(W, rows)], lsem.at[1]),
    ]
    live = length[0]
    offset = sp * rows
    rowid = lax.broadcasted_iota(jnp.int32, (128, rows), 0) // DQK
    for h in range(heads):
        tile = dqT[(h // 2) * 128:(h // 2) * 128 + 128, :]
        for m in (0, 1):
            keep = jnp.where(rowid == (h % 2) * 2 + m, 1.0, 0.0).astype(BF16)
            qz[h, m] = tile * keep
    mx[...] = jnp.full(mx.shape, NEG, F32)
    acc[...] = jnp.zeros(acc.shape, F32)

    def block(ksrc, vsrc, origin):
        spo = ring_to_sp(origin, n)
        start = spo * rows
        kpos = start + lax.broadcasted_iota(jnp.int32, (rows, 1), 0)
        klive = kpos < live
        vpos = start + lax.broadcasted_iota(jnp.int32, (1, rows), 1)
        vlive = jnp.where(vpos < live, 1.0, 0.0).astype(BF16)
        ones = jnp.broadcast_to(vlive, (16, rows))

        def head(h, carry):
            kt = ksrc[:, pl.ds(pl.multiple_of((h // 2) * 128, 128), 128)]
            vt = vsrc[pl.ds(pl.multiple_of(h * HEAD, HEAD), HEAD), :] * vlive
            vx = jnp.concatenate([vt, ones], axis=0)
            for m in (0, 1):
                for q0 in range(0, rows, 256):
                    cols = pl.ds(q0, 256)
                    s = dot(kt, qz[h, m, :, cols])
                    s = jnp.where(klive, s, NEG)
                    old = mx[h, m, :, cols]
                    new = jnp.maximum(old, jnp.max(s, axis=0, keepdims=True))
                    p = jnp.exp2(s - new).astype(BF16)
                    acc[h, m, :, cols] = acc[h, m, :, cols] * jnp.exp2(old - new) + dot(vx, p)
                    mx[h, m, :, cols] = new
            return carry

        lax.fori_loop(0, heads, head, 0)

    block(dk, dvT, me)
    for c in local[:2]:
        c.start()
    for c in local[:2]:
        c.wait()
    for c in halos:
        c.wait()

    krel = lax.broadcasted_iota(jnp.int32, (3 * W, W), 0)
    qrel = lax.broadcasted_iota(jnp.int32, (3 * W, W), 1)
    band = jnp.abs(krel - W - qrel) <= W
    krow = lax.broadcasted_iota(jnp.int32, (1, 3 * W), 1)
    zeros = jnp.zeros((HEAD, GROUP * W), BF16)

    def qblock(b, carry):
        base = offset + b * W - W
        kp = base + krel
        allowed = band & (kp >= 0) & (kp < live)
        bias = jnp.where(allowed, 0.0, NEG)
        bias = jnp.concatenate([bias] * GROUP, axis=1)
        vp = base + krow
        vlive = jnp.where((vp >= 0) & (vp < live), 1.0, 0.0).astype(BF16)
        ones = jnp.broadcast_to(vlive, (16, 3 * W))
        qlane = offset + b * W + lax.broadcasted_iota(jnp.int32, (1, W), 1)
        qlive = qlane < live
        at = pl.multiple_of(b * W, W)
        for j in range(kvh):
            lo = j * HEAD // kw * kw
            ks = kwin[pl.ds(at, 3 * W), lo:lo + kw]
            vt = vwin[j * HEAD:(j + 1) * HEAD, pl.ds(at, 3 * W)] * vlive
            vx = jnp.concatenate([vt, ones], axis=0)
            q = jnp.concatenate(
                [wqT[(j * GROUP + g) * HEAD:(j * GROUP + g + 1) * HEAD, pl.ds(at, W)] for g in range(GROUP)],
                axis=1)
            if kw > HEAD:
                q = jnp.concatenate([q, zeros] if j % 2 == 0 else [zeros, q], axis=0)
            s = dot(ks, q) + bias
            snk = jnp.concatenate(
                [jnp.full((1, W), sink[j * GROUP + g] * LOG2E, F32) for g in range(GROUP)], axis=1)
            top = jnp.maximum(snk, jnp.max(s, axis=0, keepdims=True))
            p = jnp.exp2(s - top).astype(BF16)
            o = dot(vx, p)
            r = o[:HEAD] / (o[HEAD:HEAD + 1] + jnp.exp2(snk - top))
            for g in range(GROUP):
                piece = jnp.where(qlive, r[:, g * W:(g + 1) * W], 0.0).astype(BF16)
                out[(j * GROUP + g) * HEAD:(j * GROUP + g + 1) * HEAD, pl.ds(at, W)] = piece
        return carry

    lax.fori_loop(0, rows // W, qblock, 0)

    def step(s, carry):
        kcopy(0, s).wait_recv()
        kcopy(0, s + 1).start()
        vcopy(1, s).wait_recv()
        vcopy(1, s + 1).start()
        vcopy(0, s).wait_recv()
        kcopy(1, s).wait_recv()

        @pl.when(s < half - 2)
        def _():
            vcopy(0, s + 1).start()
            kcopy(1, s + 1).start()

        def side(i, c):
            origin = (me + n + (2 * i - 1) * (s + 1)) % n
            block(kbuf.at[origin], vbuf.at[origin], origin)
            return c

        lax.fori_loop(0, 2, side, 0)
        return carry

    lax.fori_loop(0, half - 1, step, 0)
    kcopy(0, half - 1).wait_recv()
    vcopy(1, half - 1).wait_recv()
    far = (me + half) % n
    block(kbuf.at[far], vbuf.at[far], far)

    qlive = offset + lax.broadcasted_iota(jnp.int32, (1, rows), 1) < live
    base = wqT.shape[0]
    for h in range(heads):
        a0 = acc[h, 0]
        a1 = acc[h, 1]
        t0 = a0[HEAD:HEAD + 1]
        t1 = a1[HEAD:HEAD + 1]
        mixed = a0[:HEAD] / t0 - lam[h] * (a1[:HEAD] / t1)
        ms = jnp.mean(mixed * mixed, axis=0, keepdims=True)
        r = mixed * lax.rsqrt(ms + EPS) * gain[...]
        out[base + h * HEAD:base + (h + 1) * HEAD, :] = jnp.where(qlive, r, 0.0).astype(BF16)

    for d in (0, 1):
        for s in range(half):
            if s < half - 1 or d == 0:
                kcopy(d, s, s == 0).wait_send()
            if s < half - 1 or d == 1:
                vcopy(d, s, s == 0).wait_send()


def attention(n, length, sink, lam, gain, wqT, wk, wvT, dqT, dk, dvT):
    rows = wk.shape[0]
    heads = dqT.shape[0] // HEAD
    half = n // 2
    return pl.pallas_call(
        functools.partial(attention_kernel, n),
        out_shape=jax.ShapeDtypeStruct((wqT.shape[0] + dqT.shape[0], rows), BF16),
        in_specs=[SM, SM, SM] + [VM] * 7,
        out_specs=VM,
        scratch_shapes=[
            pltpu.VMEM((n,) + dk.shape, BF16),
            pltpu.VMEM((n,) + dvT.shape, BF16),
            pltpu.VMEM((rows + 2 * WINDOW, wk.shape[1]), BF16),
            pltpu.VMEM((wvT.shape[0], rows + 2 * WINDOW), BF16),
            pltpu.VMEM((heads, 2, 128, rows), BF16),
            pltpu.VMEM((heads, 2, HEAD + 16, rows), F32),
            pltpu.VMEM((heads, 2, 1, rows), F32),
            pltpu.SemaphoreType.DMA((2, 2, half)),
            pltpu.SemaphoreType.DMA((2, 2, half)),
            pltpu.SemaphoreType.DMA((2, 4)),
            pltpu.SemaphoreType.DMA((2,)),
        ],
        compiler_params=pltpu.CompilerParams(
            collective_id=1, has_side_effects=True, vmem_limit_bytes=60 * 1024 * 1024),
        name="attention",
    )(length, sink, lam, gain, wqT, wk, wvT, dqT, dk, dvT)


def body(n, inputs, length, win_query, win_key, win_value, sink_logit, diff_query, diff_key,
         diff_value, mix_lambda, head_gain, win_out, diff_out):
    seg = lax.all_gather(inputs, "tp", axis=1, tiled=True)
    wq = (dot(seg, win_query) * (HEAD ** -0.5 * LOG2E)).astype(BF16)
    wk = dot(seg, win_key).astype(BF16)
    wv = dot(seg, win_value).astype(BF16)
    dq = (dot(seg, diff_query) * (DQK ** -0.5 * LOG2E)).astype(BF16)
    dk = dot(seg, diff_key).astype(BF16)
    dv = dot(seg, diff_value).astype(BF16)
    rowsT = attention(n, length, sink_logit, mix_lambda, head_gain.reshape(-1, 1),
                      wq.T, wk, wv.T, dq.T, dk, dv.T)
    cut = win_out.shape[0]
    contract = (((0,), (0,)), ((), ()))
    part = lax.dot_general(rowsT[:cut], win_out, contract, preferred_element_type=F32)
    part += lax.dot_general(rowsT[cut:], diff_out, contract, preferred_element_type=F32)
    return lax.psum_scatter(part.astype(BF16), "tp", scatter_dimension=0, tiled=True)


def solution(mesh):
    placed = (
        P("sp", "tp"), P(), P(None, "tp"), P(None, "tp"), P(None, "tp"), P("tp"), P(None, "tp"),
        P(None, "tp"), P(None, "tp"), P("tp"), P(), P("tp", None), P("tp", None),
    )
    return jax.shard_map(
        functools.partial(body, mesh.shape["sp"]), mesh=mesh, in_specs=placed,
        out_specs=P(("sp", "tp"), None), check_vma=False)
```

time: 300 us -> 189 us (0.63)
  Pallas kernels: 0 us -> 67.5 us
  waiting for transfers between devices: 144 us -> 81.1 us
  matrix products: 84.8 us -> 24.3 us
  other arithmetic: 34.7 us -> 0 us
  local copies, waits for them, and re-layouts: 14.3 us -> 1.39 us
  starting transfers between devices: 6.77 us -> 0.04 us
    pallas_call x0 -> x1, Pallas kernels: none -> 67.5 us  [attention(): pl.pallas_call(functools.partial(attention_kernel, n), out_shape=jax.Shap...]
    all_gather x3 -> x1, waiting for transfers between devices: 99.9 us -> 36.6 us  [body(): seg = lax.all_gather(inputs, 'tp', axis=1, tiled=True)]
    dot_general x18 -> x8, matrix products: 84.8 us -> 24.3 us  [the longest x6 16.5 us: dot(): return jnp.dot(a, b, preferred_element_type=F32)]
    reduce_sum x7 -> x0, other arithmetic: 22.6 us -> none  [the longest x4 19.5 us: one_key_block(): new_total = block_sum * rescale + jnp.sum(exponent, axis=-1)]
    another operation x4 -> x0, local copies, waits for them, and re-layouts: 7.78 us -> none
    ppermute x2 -> x0, starting transfers between devices: 6.46 us -> none  [the longest x1 5.18 us: extended(): lax.ppermute(lax.slice_in_dim(block, block.shape[dim] - width, None, axis...]
    dynamic_update_slice x8 -> x0, other arithmetic: 5.22 us -> none  [the longest x4 5.14 us: one_query_block(): lax.dynamic_update_slice_in_dim(total_sum, final_state[1], row_begin, 2)]
    while x16 -> x0, local copies, waits for them, and re-layouts: 3.37 us -> none
  transfers between devices with their start and end apart: 6 -> 2, of which waited for: 4 -> 2; matrix products, arithmetic and copies ran while one was open for 10% -> 1% of each run, Pallas kernels for 0% -> 0%
where the time goes in v1:
time: 189 us
  waiting for transfers between devices  81.1 us (43%)
  Pallas kernels  67.5 us (36%)
  matrix products  24.3 us (13%)
  between operations  14.3 us (8%)
    pallas_call x1, Pallas kernels, attention(): pl.pallas_call(functools.partial(attention_kernel, n), out_shape=jax.Shap...  67.5 us
    reduce_scatter x1, waiting for transfers between devices, body(): lax.psum_scatter(part.astype(BF16), 'tp', scatter_dimension=0, tiled=True)  43.8 us
    all_gather x1, waiting for transfers between devices, body(): seg = lax.all_gather(inputs, 'tp', axis=1, tiled=True)  36.6 us
    dot_general x6, matrix products, dot(): return jnp.dot(a, b, preferred_element_type=F32)  16.5 us
    dot_general x1, matrix products, body(): lax.dot_general(rowsT[cut:], diff_out, contract, preferred_element_type=F32)  4.2 us
  transfers between devices with their start and end apart: 2, of which 2 were waited for; matrix products, arithmetic and copies ran while one was open for 1% of the time, Pallas kernels for 0%

profile of v1, /device:TPU:0, one launch (start us, length us, event | category | flops | bytes accessed | tf_op | source)
XLA Modules:
  0.0 188.6 jit_solution(7781993427098247670)
XLA Ops:
  6.5 0.0 copy-start
  6.5 0.0 all-gather.2.cloned.1.call-start
  6.5 0.7 all-gather.2.cloned.1.call-update
  7.3 0.0 reduce-scatter.2.cloned.1.call-start
  8.1 1.4 copy.14.gain
  9.5 36.6 %all-gather.2.cloned.1.call-done = bf16[512,4096]{1,0:T(8,128)(2,1)} async-done(((bf16[512,1024]{1,0:T(8,128)(2,1)}), bf16[512,4096]{1,0:T(8,128)(2,1)}) %all-gather.2.cloned.1.call-update) | async-done | bytes 4194320 | tf_op jit(solution)/shard_map/all_gather | solution.py:256
  46.1 0.0 copy-start.1
  46.1 0.0 copy-start.4
  46.1 4.8 %convolution_convert_fusion.2.wvT = bf16[128,512]{1,0:T(8,128)(2,1)} fusion(bf16[4096,128]{1,0:T(8,128)(2,1)} %param.17, bf16[512,4096]{1,0:T(8,128)(2,1)} %all-gather.2.cloned.1.call-done), kind=kOutput, calls=%fused_computation.7 | convolution fusion | flops 536936448 | bytes 5373952 | tf_op jit(solution)/shard_map/dot_general | solution.py:25
  51.0 0.0 copy-done.1
  51.0 3.1 %convolution_convert_fusion.3.wk = bf16[512,128]{1,0:T(8,128)(2,1)} fusion(bf16[512,4096]{1,0:T(8,128)(2,1)S(1)} %copy-done.1, bf16[4096,128]{1,0:T(8,128)(2,1)} %param.16), kind=kOutput, calls=%fused_computation.8 | convolution fusion | flops 536936448 | bytes 5373952 | tf_op jit(solution)/shard_map/dot_general | solution.py:25
  54.1 0.0 copy-done.4
  54.1 0.0 copy-start.5
  54.1 2.0 %convolution_convert_fusion.dvT = bf16[256,512]{1,0:T(8,128)(2,1)} fusion(bf16[4096,256]{1,0:T(8,128)(2,1)S(1)} %copy-done.4, bf16[512,4096]{1,0:T(8,128)(2,1)S(1)} %copy-done.1), kind=kOutput, calls=%fused_computation.5 | convolution fusion | flops 1073872896 | bytes 6553600 | tf_op jit(solution)/shard_map/dot_general | solution.py:25
  56.1 0.0 copy-done.5
  56.1 0.0 copy-start.6
  56.1 2.0 %convolution_convert_fusion.1.dk = bf16[512,256]{1,0:T(8,128)(2,1)} fusion(bf16[512,4096]{1,0:T(8,128)(2,1)S(1)} %copy-done.1, bf16[4096,256]{1,0:T(8,128)(2,1)S(1)} %copy-done.5), kind=kOutput, calls=%fused_computation.6 | convolution fusion | flops 1073872896 | bytes 6553600 | tf_op jit(solution)/shard_map/dot_general | solution.py:25
  58.0 0.0 copy-done.6
  58.0 0.0 copy-start.3
  58.0 2.0 %fusion.1.dqT = bf16[256,512]{1,0:T(8,128)(2,1)} fusion(bf16[4096,256]{1,0:T(8,128)(2,1)S(1)} %copy-done.6, bf16[512,4096]{1,0:T(8,128)(2,1)S(1)} %copy-done.1), kind=kOutput, calls=%fused_computation.4 | convolution fusion | flops 1074003968 | bytes 6553600 | tf_op jit(solution)/shard_map/dot_general | solution.py:25
  60.1 0.0 copy-done.3
  60.1 2.6 %fusion.wqT = bf16[384,512]{1,0:T(8,128)(2,1)} fusion(bf16[4096,384]{1,0:T(8,128)(2,1)S(1)} %copy-done.3, bf16[512,4096]{1,0:T(8,128)(2,1)S(1)} %copy-done.1), kind=kOutput, calls=%fused_computation.2 | convolution fusion | flops 1611005952 | bytes 7733248 | tf_op jit(solution)/shard_map/dot_general | solution.py:25
  62.7 67.5 %attention.1 = bf16[640,512]{1,0:T(8,128)(2,1)} custom-call(s32[1]{0:T(128)S(6)} %copy.15.length, f32[6]{0:T(128)} %sink.1, f32[4]{0:T(128)} %lam.1, f32[64,1]{1,0:T(8,128)} %copy.14.gain, bf16[384,512]{1,0:T(8,128)(2,1)} %fusion.wqT, bf16[512,128]{1,0:T(8,128)(2,1)} %convolution_convert_fusion.3.wk, bf16[128,512]{1,0:T(8,128)(2,1)} %convolution_convert_fusion.2.wvT, ...), custom_call_target="tpu_custom_call" | custom-call | tf_op jit(solution)/shard_map/attention/pallas_call | solution.py:230
  130.2 0.0 copy-done
  130.2 0.0 copy-start.2
  130.2 3.5 %fusion.2 = f32[512,4096]{1,0:T(8,128)S(1)} fusion(bf16[384,4096]{1,0:T(8,128)(2,1)S(1)} %copy-done, bf16[640,512]{1,0:T(8,128)(2,1)} %attention.1), kind=kOutput, calls=%fused_computation.9 | convolution fusion | flops 1610612736 | bytes 11927552 | tf_op jit(solution)/shard_map/dot_general | solution.py:267
  133.7 0.0 copy-done.2
  133.8 4.2 %add_convert_fusion = bf16[512,4096]{1,0:T(8,128)(2,1)} fusion(f32[512,4096]{1,0:T(8,128)S(1)} %fusion.2, bf16[256,4096]{1,0:T(8,128)(2,1)S(1)} %copy-done.2, bf16[640,512]{1,0:T(8,128)(2,1)} %attention.1), kind=kOutput, calls=%fused_computation | convolution fusion | flops 1077936128 | bytes 14942208 | tf_op jit(solution)/shard_map/dot_general | solution.py:268
  138.0 0.0 reduce-scatter.2.cloned.1.call-update
  138.0 43.8 %reduce-scatter.2.cloned.1.call-done = bf16[128,4096]{1,0:T(8,128)(2,1)} async-done(((bf16[512,4096]{1,0:T(8,128)(2,1)}), bf16[128,4096]{1,0:T(8,128)(2,1)}) %reduce-scatter.2.cloned.1.call-update) | async-done | bytes 1048592 | tf_op jit(solution)/shard_map/reduce_scatter | solution.py:269
Async XLA Ops:
  6.5 123.7 %copy-start = (bf16[384,4096]{1,0:T(8,128)(2,1)S(1)}, bf16[384,4096]{1,0:T(8,128)(2,1)}, u32[]{:S(2)}) copy-start(bf16[384,4096]{1,0:T(8,128)(2,1)} %param.24) | copy-start | bytes 9437188
  6.5 39.6 %all-gather.2.cloned.1.call-start = ((), (), s32[]{:S(2)}) async-start(), calls=%async_computation.1 | async-start | bytes 5242880 | tf_op jit(solution)/shard_map/all_gather | solution.py:256
  7.3 174.5 %reduce-scatter.2.cloned.1.call-start = ((), (), s32[]{:S(2)}) async-start(), calls=%async_computation.2 | async-start | bytes 5242880 | tf_op jit(solution)/shard_map/reduce_scatter | solution.py:269
  46.1 4.8 %copy-start.1 = (bf16[512,4096]{1,0:T(8,128)(2,1)S(1)}, bf16[512,4096]{1,0:T(8,128)(2,1)}, u32[]{:S(2)}) copy-start(bf16[512,4096]{1,0:T(8,128)(2,1)} %all-gather.2.cloned.1.call-done) | copy-start | bytes 12582916
  46.1 8.0 %copy-start.4 = (bf16[4096,256]{1,0:T(8,128)(2,1)S(1)}, bf16[4096,256]{1,0:T(8,128)(2,1)}, u32[]{:S(2)}) copy-start(bf16[4096,256]{1,0:T(8,128)(2,1)} %param.21) | copy-start | bytes 6291460
  54.1 2.0 %copy-start.5 = (bf16[4096,256]{1,0:T(8,128)(2,1)S(1)}, bf16[4096,256]{1,0:T(8,128)(2,1)}, u32[]{:S(2)}) copy-start(bf16[4096,256]{1,0:T(8,128)(2,1)} %param.20) | copy-start | bytes 6291460
  56.1 2.0 %copy-start.6 = (bf16[4096,256]{1,0:T(8,128)(2,1)S(1)}, bf16[4096,256]{1,0:T(8,128)(2,1)}, u32[]{:S(2)}) copy-start(bf16[4096,256]{1,0:T(8,128)(2,1)} %param.19) | copy-start | bytes 6291460
  58.0 2.0 %copy-start.3 = (bf16[4096,384]{1,0:T(8,128)(2,1)S(1)}, bf16[4096,384]{1,0:T(8,128)(2,1)}, u32[]{:S(2)}) copy-start(bf16[4096,384]{1,0:T(8,128)(2,1)} %param.15) | copy-start | bytes 9437188
  130.2 3.5 %copy-start.2 = (bf16[256,4096]{1,0:T(8,128)(2,1)S(1)}, bf16[256,4096]{1,0:T(8,128)(2,1)}, u32[]{:S(2)}) copy-start(bf16[256,4096]{1,0:T(8,128)(2,1)} %param.25) | copy-start | bytes 6291460
Sparse Core Ops, SparseCore 0:
  8.9 37.1 all-gather.1
  138.1 43.6 reduce-scatter.1

commit v2 on v1

--- a/solution.py
+++ b/solution.py
@@ -16,6 +16,7 @@
 EPS = 1e-06
 MESH = pl.DeviceIdType.MESH
 VM = pl.BlockSpec(memory_space=pltpu.VMEM)
+ANY = pl.BlockSpec(memory_space=pl.ANY)
 SM = pl.BlockSpec(memory_space=pltpu.SMEM)
 F32 = jnp.float32
 BF16 = jnp.bfloat16
@@ -31,8 +32,8 @@
 
 
 def attention_kernel(
-    n, length, sink, lam, gain, wqT, wk, wvT, dqT, dk, dvT,
-    out, kbuf, vbuf, kwin, vwin, qz, acc, mx, ksem, vsem, hsem, lsem,
+    n, length, sink, lam, gain, wqT, wk, wvT, dqT, dk, dvT, wo, do,
+    out_rows, wpeer, out, kbuf, vbuf, kwin, vwin, qz, acc, mx, ksem, vsem, hsem, lsem, wsem,
 ):
     rows = wk.shape[0]
     heads = dqT.shape[0] // HEAD
@@ -50,7 +51,10 @@
     barrier = pltpu.get_barrier_semaphore()
     for d in (left, right, prv, nxt):
         pl.semaphore_signal(barrier, inc=1, device_id={"sp": d}, device_id_type=MESH)
-    pl.semaphore_wait(barrier, 4)
+    tp = lax.axis_index("tp")
+    peer = tp + 1 - 2 * (tp % 2)
+    pl.semaphore_signal(barrier, inc=1, device_id={"tp": peer}, device_id_type=MESH)
+    pl.semaphore_wait(barrier, 5)
 
     W = WINDOW
     halos = []
@@ -83,6 +87,16 @@
     for d in (0, 1):
         kcopy(d, 0, True).start()
         vcopy(d, 0, True).start()
+
+    cut = wo.shape[0]
+    shared = [
+        pltpu.make_async_remote_copy(
+            src_ref=src, dst_ref=wpeer.at[pl.ds(at, src.shape[0])], send_sem=wsem.at[0, i],
+            recv_sem=wsem.at[1, i], device_id={"tp": peer}, device_id_type=MESH)
+        for i, (src, at) in enumerate(((wo, 0), (do, cut)))
+    ]
+    for c in shared:
+        c.start()
 
     local = [
         pltpu.make_async_copy(wk, kwin.at[pl.ds(W, rows)], lsem.at[0]),
@@ -215,24 +229,36 @@
         r = mixed * lax.rsqrt(ms + EPS) * gain[...]
         out[base + h * HEAD:base + (h + 1) * HEAD, :] = jnp.where(qlive, r, 0.0).astype(BF16)
 
+    hidden = out.shape[0]
+    for c0 in range(0, hidden, 128):
+        w = min(128, hidden - c0)
+        out_rows[:, c0:c0 + w] = out[c0:c0 + w, :].T
+
     for d in (0, 1):
         for s in range(half):
             if s < half - 1 or d == 0:
                 kcopy(d, s, s == 0).wait_send()
             if s < half - 1 or d == 1:
                 vcopy(d, s, s == 0).wait_send()
-
-
-def attention(n, length, sink, lam, gain, wqT, wk, wvT, dqT, dk, dvT):
+    for c in shared:
+        c.wait()
+
+
+def attention(n, length, sink, lam, gain, wqT, wk, wvT, dqT, dk, dvT, wo, do):
+    hidden = wqT.shape[0] + dqT.shape[0]
     rows = wk.shape[0]
     heads = dqT.shape[0] // HEAD
     half = n // 2
     return pl.pallas_call(
         functools.partial(attention_kernel, n),
-        out_shape=jax.ShapeDtypeStruct((wqT.shape[0] + dqT.shape[0], rows), BF16),
-        in_specs=[SM, SM, SM] + [VM] * 7,
-        out_specs=VM,
+        out_shape=(
+            jax.ShapeDtypeStruct((rows, hidden), BF16),
+            jax.ShapeDtypeStruct((hidden, wo.shape[1]), BF16),
+        ),
+        in_specs=[SM, SM, SM] + [VM] * 7 + [ANY] * 2,
+        out_specs=(VM, ANY),
         scratch_shapes=[
+            pltpu.VMEM((hidden, rows), BF16),
             pltpu.VMEM((n,) + dk.shape, BF16),
             pltpu.VMEM((n,) + dvT.shape, BF16),
             pltpu.VMEM((rows + 2 * WINDOW, wk.shape[1]), BF16),
@@ -244,29 +270,237 @@
             pltpu.SemaphoreType.DMA((2, 2, half)),
             pltpu.SemaphoreType.DMA((2, 4)),
             pltpu.SemaphoreType.DMA((2,)),
+            pltpu.SemaphoreType.DMA((2, 2)),
         ],
         compiler_params=pltpu.CompilerParams(
             collective_id=1, has_side_effects=True, vmem_limit_bytes=60 * 1024 * 1024),
         name="attention",
-    )(length, sink, lam, gain, wqT, wk, wvT, dqT, dk, dvT)
-
-
-def body(n, inputs, length, win_query, win_key, win_value, sink_logit, diff_query, diff_key,
+    )(length, sink, lam, gain, wqT, wk, wvT, dqT, dk, dvT, wo, do)
+
+
+def gather_kernel(
+    xs, widths, x, *refs,
+):
+    weights = refs[:-13]
+    wqT, wk, wvT, dqT, dk, dvT, seg, wbuf, acc, wsem, psem, xsem, rsem = refs[-13:]
+    rows, feats = x.shape
+    step_rows = 128
+    steps = rows // step_rows
+    tp = lax.axis_index("tp")
+    core = tp % 2
+    xi = tp // 2
+    peer = xi * 2 + 1 - core
+    others = [((xi + d) % xs) * 2 + core for d in range(1, xs)]
+    barrier = pltpu.get_barrier_semaphore()
+    for d in others + [peer]:
+        pl.semaphore_signal(barrier, inc=1, device_id={"tp": d}, device_id_type=MESH)
+    pl.semaphore_wait(barrier, xs)
+
+    def across(c, d):
+        part = pl.ds(pl.multiple_of(c * step_rows, step_rows), step_rows)
+        return pltpu.make_async_remote_copy(
+            src_ref=x.at[part], dst_ref=seg.at[tp, part], send_sem=xsem.at[0, d, c],
+            recv_sem=xsem.at[1, d, c], device_id={"tp": others[d]}, device_id_type=MESH)
+
+    def relay(c, d):
+        source = ((xi + xs - d - 1) % xs) * 2 + core
+        part = pl.ds(pl.multiple_of(c * step_rows, step_rows), step_rows)
+        return pltpu.make_async_remote_copy(
+            src_ref=seg.at[source, part], dst_ref=seg.at[source, part], send_sem=rsem.at[0, d, c],
+            recv_sem=rsem.at[1, d, c], device_id={"tp": peer}, device_id_type=MESH)
+
+    for c in range(steps):
+        for d in range(xs - 1):
+            across(c, d).start()
+    beside = pltpu.make_async_remote_copy(
+        src_ref=x, dst_ref=seg.at[tp], send_sem=psem.at[0], recv_sem=psem.at[1],
+        device_id={"tp": peer}, device_id_type=MESH)
+    beside.start()
+    loads, at = [], 0
+    for i, w in enumerate(weights):
+        loads.append(pltpu.make_async_copy(w, wbuf.at[:, pl.ds(at, w.shape[1])], wsem.at[i]))
+        at += w.shape[1]
+    cuts = [(sum(widths[:i]), sum(widths[:i + 1])) for i in range(6)]
+    for c in loads:
+        c.start()
+    for c in loads:
+        c.wait()
+    beside.wait_recv()
+
+    def weight(t):
+        return wbuf[pl.ds(pl.multiple_of(t * feats, feats), feats), :]
+
+    def near(c, carry):
+        part = pl.ds(pl.multiple_of(c * step_rows, step_rows), step_rows)
+        acc[part, :] = dot(x[part, :], weight(tp)) + dot(seg[peer, part, :], weight(peer))
+        return carry
+
+    lax.fori_loop(0, steps, near, 0)
+
+    def far(c, carry):
+        part = pl.ds(pl.multiple_of(c * step_rows, step_rows), step_rows)
+        total = acc[part, :]
+        for d in range(xs - 1):
+            source = (xi + xs - d - 1) % xs
+            across(c, d).wait_recv()
+            relay(c, d).start()
+            total += dot(seg[source * 2 + core, part, :], weight(source * 2 + core))
+            relay(c, d).wait_recv()
+            total += dot(seg[source * 2 + 1 - core, part, :], weight(source * 2 + 1 - core))
+        pieces = [total[:, a:b] for a, b in cuts]
+        wqT[:, part] = (pieces[0] * (HEAD ** -0.5 * LOG2E)).T.astype(BF16)
+        wk[part, :] = pieces[1].astype(BF16)
+        wvT[:, part] = pieces[2].T.astype(BF16)
+        dqT[:, part] = (pieces[3] * (DQK ** -0.5 * LOG2E)).T.astype(BF16)
+        dk[part, :] = pieces[4].astype(BF16)
+        dvT[:, part] = pieces[5].T.astype(BF16)
+        return carry
+
+    lax.fori_loop(0, steps, far, 0)
+    beside.wait_send()
+    for c in range(steps):
+        for d in range(xs - 1):
+            across(c, d).wait_send()
+            relay(c, d).wait_send()
+
+
+def gather(xs, x, *weights):
+    rows, feats = x.shape
+    widths = [w.shape[1] for w in weights]
+    steps = rows // 128
+    depth = weights[0].shape[0]
+    if any(w % 128 for w in widths):
+        weights = [jnp.concatenate(weights, axis=1)]
+    shapes = [(widths[0], rows), (rows, widths[1]), (widths[2], rows),
+              (widths[3], rows), (rows, widths[4]), (widths[5], rows)]
+    return pl.pallas_call(
+        functools.partial(gather_kernel, xs, widths),
+        out_shape=[jax.ShapeDtypeStruct(s, BF16) for s in shapes],
+        in_specs=[VM] + [ANY] * len(weights),
+        out_specs=[VM] * 6,
+        scratch_shapes=[
+            pltpu.VMEM((2 * xs, rows, feats), BF16),
+            pltpu.VMEM((depth, sum(widths)), BF16),
+            pltpu.VMEM((rows, sum(widths)), F32),
+            pltpu.SemaphoreType.DMA((6,)),
+            pltpu.SemaphoreType.DMA((2,)),
+            pltpu.SemaphoreType.DMA((2, xs - 1, steps)),
+            pltpu.SemaphoreType.DMA((2, xs - 1, steps)),
+        ],
+        compiler_params=pltpu.CompilerParams(
+            collective_id=2, has_side_effects=True, vmem_limit_bytes=60 * 1024 * 1024),
+        name="gather",
+    )(x, *weights)
+
+
+def project_kernel(xs, parts, a, wo, do, wp, out, wbuf, ap, sbuf, rbuf, wsem, asem, ssem):
+    rows, hidden = a.shape
+    share = rows // (2 * xs)
+    width = out.shape[1] // parts
+    tp = lax.axis_index("tp")
+    core = tp % 2
+    xi = tp // 2
+    peer = xi * 2 + 1 - core
+    others = [((xi + d) % xs) * 2 + core for d in range(1, xs)]
+    cut = wo.shape[0]
+
+    def loads(j):
+        cols = pl.ds(pl.multiple_of(j * width, width), width)
+        return [
+            pltpu.make_async_copy(src.at[:, cols], wbuf.at[pl.ds(at, src.shape[0]), cols], wsem.at[j, i])
+            for i, (src, at) in enumerate(((wo, 0), (do, cut), (wp, hidden)))
+        ]
+
+    for j in range(parts):
+        for c in loads(j):
+            c.start()
+    barrier = pltpu.get_barrier_semaphore()
+    for d in others + [peer]:
+        pl.semaphore_signal(barrier, inc=1, device_id={"tp": d}, device_id_type=MESH)
+    pl.semaphore_wait(barrier, xs)
+
+    def rows_of(block):
+        return pl.ds(pl.multiple_of(block * share, share), share)
+
+    swaps = [
+        pltpu.make_async_remote_copy(
+            src_ref=a.at[rows_of(c * 2 + 1 - core)], dst_ref=ap.at[c], send_sem=asem.at[0, c],
+            recv_sem=asem.at[1, c], device_id={"tp": peer}, device_id_type=MESH)
+        for c in range(xs)
+    ]
+    for c in swaps:
+        c.start()
+    for c in swaps:
+        c.wait()
+
+    def send(j, d):
+        cols = pl.ds(pl.multiple_of(j * width, width), width)
+        return pltpu.make_async_remote_copy(
+            src_ref=sbuf.at[d, :, cols], dst_ref=rbuf.at[d, :, cols], send_sem=ssem.at[0, d, j],
+            recv_sem=ssem.at[1, d, j], device_id={"tp": others[d]}, device_id_type=MESH)
+
+    def product(chip, cols):
+        lhs = jnp.concatenate([a[rows_of(chip * 2 + core), :], ap[chip]], axis=1)
+        return dot(lhs, wbuf[:, cols])
+
+    def remote(j, carry):
+        for c in loads(j):
+            c.wait()
+        cols = pl.ds(pl.multiple_of(j * width, width), width)
+        for d in range(xs - 1):
+            sbuf[d, :, cols] = product((xi + d + 1) % xs, cols).astype(BF16)
+            send(j, d).start()
+        return carry
+
+    lax.fori_loop(0, parts, remote, 0)
+
+    def own(j, carry):
+        cols = pl.ds(pl.multiple_of(j * width, width), width)
+        total = product(xi, cols)
+        for d in range(xs - 1):
+            send(j, d).wait_recv()
+            total += rbuf[d, :, cols].astype(F32)
+        out[:, cols] = total.astype(BF16)
+        return carry
+
+    lax.fori_loop(0, parts, own, 0)
+    for j in range(parts):
+        for d in range(xs - 1):
+            send(j, d).wait_send()
+
+
+def project(xs, a, wo, do, wp):
+    rows, hidden = a.shape
+    share = rows // (2 * xs)
+    model = wo.shape[1]
+    parts = 8
+    return pl.pallas_call(
+        functools.partial(project_kernel, xs, parts),
+        out_shape=jax.ShapeDtypeStruct((share, model), BF16),
+        in_specs=[VM] + [ANY] * 3,
+        out_specs=VM,
+        scratch_shapes=[
+            pltpu.VMEM((2 * hidden, model), BF16),
+            pltpu.VMEM((xs, share, hidden), BF16),
+            pltpu.VMEM((xs - 1, share, model), BF16),
+            pltpu.VMEM((xs - 1, share, model), BF16),
+            pltpu.SemaphoreType.DMA((parts, 3)),
+            pltpu.SemaphoreType.DMA((2, xs)),
+            pltpu.SemaphoreType.DMA((2, xs - 1, parts)),
+        ],
+        compiler_params=pltpu.CompilerParams(
+            collective_id=3, has_side_effects=True, vmem_limit_bytes=60 * 1024 * 1024),
+        name="project",
+    )(a, wo, do, wp)
+
+
+def body(n, xs, inputs, length, win_query, win_key, win_value, sink_logit, diff_query, diff_key,
          diff_value, mix_lambda, head_gain, win_out, diff_out):
-    seg = lax.all_gather(inputs, "tp", axis=1, tiled=True)
-    wq = (dot(seg, win_query) * (HEAD ** -0.5 * LOG2E)).astype(BF16)
-    wk = dot(seg, win_key).astype(BF16)
-    wv = dot(seg, win_value).astype(BF16)
-    dq = (dot(seg, diff_query) * (DQK ** -0.5 * LOG2E)).astype(BF16)
-    dk = dot(seg, diff_key).astype(BF16)
-    dv = dot(seg, diff_value).astype(BF16)
-    rowsT = attention(n, length, sink_logit, mix_lambda, head_gain.reshape(-1, 1),
-                      wq.T, wk, wv.T, dq.T, dk, dv.T)
-    cut = win_out.shape[0]
-    contract = (((0,), (0,)), ((), ()))
-    part = lax.dot_general(rowsT[:cut], win_out, contract, preferred_element_type=F32)
-    part += lax.dot_general(rowsT[cut:], diff_out, contract, preferred_element_type=F32)
-    return lax.psum_scatter(part.astype(BF16), "tp", scatter_dimension=0, tiled=True)
+    wqT, wk, wvT, dqT, dk, dvT = gather(
+        xs, inputs, win_query, win_key, win_value, diff_query, diff_key, diff_value)
+    rows, wp = attention(n, length, sink_logit, mix_lambda, head_gain.reshape(-1, 1),
+                         wqT, wk, wvT, dqT, dk, dvT, win_out, diff_out)
+    return project(xs, rows, win_out, diff_out, wp)
 
 
 def solution(mesh):
@@ -275,5 +509,5 @@
         P(None, "tp"), P(None, "tp"), P("tp"), P(), P("tp", None), P("tp", None),
     )
     return jax.shard_map(
-        functools.partial(body, mesh.shape["sp"]), mesh=mesh, in_specs=placed,
+        functools.partial(body, mesh.shape["sp"], mesh.shape["tp"] // 2), mesh=mesh, in_specs=placed,
         out_specs=P(("sp", "tp"), None), check_vma=False)

time: 189 us -> 134 us (0.71)
  waiting for transfers between devices: 81.1 us -> 0 us
  Pallas kernels: 67.5 us -> 130 us
  matrix products: 24.3 us -> 0 us
  between operations: 14.3 us -> 0.68 us
  local copies, waits for them, and re-layouts: 1.39 us -> 3.65 us
    pallas_call x1 -> x3, Pallas kernels: 67.5 us -> 130 us  [the longest x1 68.6 us: attention(): pl.pallas_call(functools.partial(attention_kernel, n), out_shape=(jax.Sha...]
    reduce_scatter x1 -> x0, waiting for transfers between devices: 43.8 us -> none  [body(): lax.psum_scatter(part.astype(BF16), 'tp', scatter_dimension=0, tiled=True)]
    all_gather x1 -> x0, waiting for transfers between devices: 36.6 us -> none  [body(): seg = lax.all_gather(inputs, 'tp', axis=1, tiled=True)]
    dot_general x8 -> x0, matrix products: 24.3 us -> none  [the longest x6 16.5 us: dot(): return jnp.dot(a, b, preferred_element_type=F32)]
    unnamed x14 -> x1, local copies, waits for them, and re-layouts: 0.03 us -> 2.29 us
  transfers between devices with their start and end apart: 2 -> 0, of which waited for: 2 -> 0; matrix products, arithmetic and copies ran while one was open for 1% -> 0% of each run, Pallas kernels for 0% -> 0%
where the time goes in v2:
time: 134 us
  Pallas kernels  130 us (97%)
  local copies, waits for them, and re-layouts  3.65 us (3%)
    pallas_call x1, Pallas kernels, attention(): pl.pallas_call(functools.partial(attention_kernel, n), out_shape=(jax.Sha...  68.6 us
    pallas_call x1, Pallas kernels, gather(): pl.pallas_call(functools.partial(gather_kernel, xs, widths), out_shape=[j...  31 us
    pallas_call x1, Pallas kernels, project(): pl.pallas_call(functools.partial(project_kernel, xs, parts), out_shape=ja...  30.2 us

profile of v2, /device:TPU:0, one launch (start us, length us, event | category | flops | bytes accessed | tf_op | source)
XLA Modules:
  0.0 134.1 jit_solution(16652945763778394151)
XLA Ops:
  0.7 1.4 %copy.14.gain = f32[64,1]{1,0:T(8,128)} copy(f32[64,1]{0,1:T(1,128)} %bitcast.1) | data formatting | bytes 512 | tf_op jit(solution)/shard_map/reshape | solution.py:501
  2.0 31.0 %gather.1 = (bf16[384,512]{1,0:T(8,128)(2,1)}, bf16[512,128]{1,0:T(8,128)(2,1)}, bf16[128,512]{1,0:T(8,128)(2,1)}, bf16[256,512]{1,0:T(8,128)(2,1)}, bf16[512,256]{1,0:T(8,128)(2,1)}, /*index=5*/bf16[256,512]{1,0:T(8,128)(2,1)}) custom-call(bf16[512,1024]{1,0:T(8,128)(2,1)} %x.1, bf16[4096,384]{1,0:T(8,128)(2,1)} %refs_0_.1, bf16[4096,128]{1,0:T(8,128)(2,1)} %refs_1_.1, ...), custom_call_target="tpu_custom_call" | custom-call | tf_op jit(solution)/shard_map/gather/pallas_call | solution.py:376
  33.0 68.6 %attention.1 = (bf16[512,640]{1,0:T(8,128)(2,1)}, bf16[640,4096]{1,0:T(8,128)(2,1)}) custom-call(s32[1]{0:T(128)S(6)} %copy.16.length, f32[6]{0:T(128)} %sink.1, f32[4]{0:T(128)} %lam.1, f32[64,1]{1,0:T(8,128)} %copy.14.gain, bf16[384,512]{1,0:T(8,128)(2,1)} %get-tuple-element.13.wqT, bf16[512,128]{1,0:T(8,128)(2,1)} %get-tuple-element.14.wk, ...), custom_call_target="tpu_custom_call" | custom-call | tf_op jit(solution)/shard_map/attention/pallas_call | solution.py:252
  101.6 30.2 %project.1 = bf16[128,4096]{1,0:T(8,128)(2,1)} custom-call(bf16[512,640]{1,0:T(8,128)(2,1)} %get-tuple-element.19.a, bf16[384,4096]{1,0:T(8,128)(2,1)} %wo.3, bf16[256,4096]{1,0:T(8,128)(2,1)} %do.3, bf16[640,4096]{1,0:T(8,128)(2,1)} %get-tuple-element.20.wp), custom_call_target="tpu_custom_call" | custom-call | tf_op jit(solution)/shard_map/project/pallas_call | solution.py:477
  131.8 2.3 %copy.17 = bf16[128,4096]{1,0:T(8,128)(2,1)} copy(bf16[128,4096]{1,0:T(8,128)(2,1)} %project.1) | data formatting | bytes 2097152

commit v3 on v2

--- a/solution.py
+++ b/solution.py
@@ -31,14 +31,21 @@
     return (1 - half) * (2 * r) + half * (2 * (n - 1 - r) + 1)
 
 
-def attention_kernel(
-    n, length, sink, lam, gain, wqT, wk, wvT, dqT, dk, dvT, wo, do,
-    out_rows, wpeer, out, kbuf, vbuf, kwin, vwin, qz, acc, mx, ksem, vsem, hsem, lsem, wsem,
-):
-    rows = wk.shape[0]
+def layer_kernel(n, xs, widths, length, sink, lam, gain, x, *refs):
+    weights = refs[:-31]
+    (wo, do, out_rows, wpeer, wqT, wk, wvT, dqT, dk, dvT, seg, wbuf, pacc, out, kbuf, vbuf, kwin, vwin, qz,
+     acc, mx, ldsem, psem, xsem, rsem, csem, ksem, vsem, hsem, lsem, wsem) = refs[-31:]
+    rows, feats = x.shape
+    step_rows = 128
+    steps = rows // step_rows
     heads = dqT.shape[0] // HEAD
     kvh = wk.shape[1] // HEAD
     kw = min(2 * HEAD, wk.shape[1])
+    tp = lax.axis_index("tp")
+    core = tp % 2
+    xi = tp // 2
+    peer = xi * 2 + 1 - core
+    others = [((xi + d) % xs) * 2 + core for d in range(1, xs)]
     sp = lax.axis_index("sp")
     y = sp % 2
     z = sp // 2
@@ -48,15 +55,113 @@
     left = ring_to_sp((me + n - 1) % n, n)
     nxt = (sp + 1) % n
     prv = (sp + n - 1) % n
+    W = WINDOW
     barrier = pltpu.get_barrier_semaphore()
     for d in (left, right, prv, nxt):
         pl.semaphore_signal(barrier, inc=1, device_id={"sp": d}, device_id_type=MESH)
-    tp = lax.axis_index("tp")
-    peer = tp + 1 - 2 * (tp % 2)
-    pl.semaphore_signal(barrier, inc=1, device_id={"tp": peer}, device_id_type=MESH)
-    pl.semaphore_wait(barrier, 5)
-
-    W = WINDOW
+    for d in others + [peer]:
+        pl.semaphore_signal(barrier, inc=1, device_id={"tp": d}, device_id_type=MESH)
+    pl.semaphore_wait(barrier, 4 + xs)
+
+    def first(kind, direction, c):
+        part = pl.ds(pl.multiple_of(c * step_rows, step_rows), step_rows)
+        src, dst = ((dk.at[part], kbuf.at[me, part]), (dvT.at[:, part], vbuf.at[me, :, part]))[kind]
+        return pltpu.make_async_remote_copy(
+            src_ref=src, dst_ref=dst, send_sem=csem.at[0, kind, direction, c],
+            recv_sem=csem.at[1, kind, direction, c],
+            device_id={"sp": (right, left)[direction]}, device_id_type=MESH)
+
+    def hop(kind, direction, s):
+        slot = (me + n - s) % n if direction == 0 else (me + s) % n
+        buf, sem = ((kbuf, ksem), (vbuf, vsem))[kind]
+        return pltpu.make_async_remote_copy(
+            src_ref=buf.at[slot], dst_ref=buf.at[slot],
+            send_sem=sem.at[0, direction, s], recv_sem=sem.at[1, direction, s],
+            device_id={"sp": (right, left)[direction]}, device_id_type=MESH)
+
+    def arrived(kind, direction, s):
+        if isinstance(s, int):
+            if s == 0:
+                for c in range(steps):
+                    first(kind, direction, c).wait_recv()
+            else:
+                hop(kind, direction, s).wait_recv()
+            return
+
+        @pl.when(s == 0)
+        def _():
+            for c in range(steps):
+                first(kind, direction, c).wait_recv()
+
+        @pl.when(s > 0)
+        def _():
+            hop(kind, direction, s).wait_recv()
+
+    def across(c, d):
+        part = pl.ds(pl.multiple_of(c * step_rows, step_rows), step_rows)
+        return pltpu.make_async_remote_copy(
+            src_ref=x.at[part], dst_ref=seg.at[tp, part], send_sem=xsem.at[0, d, c],
+            recv_sem=xsem.at[1, d, c], device_id={"tp": others[d]}, device_id_type=MESH)
+
+    def relay(c, d):
+        source = ((xi + xs - d - 1) % xs) * 2 + core
+        part = pl.ds(pl.multiple_of(c * step_rows, step_rows), step_rows)
+        return pltpu.make_async_remote_copy(
+            src_ref=seg.at[source, part], dst_ref=seg.at[source, part], send_sem=rsem.at[0, d, c],
+            recv_sem=rsem.at[1, d, c], device_id={"tp": peer}, device_id_type=MESH)
+
+    for c in range(steps):
+        for d in range(xs - 1):
+            across(c, d).start()
+    beside = pltpu.make_async_remote_copy(
+        src_ref=x, dst_ref=seg.at[tp], send_sem=psem.at[0], recv_sem=psem.at[1],
+        device_id={"tp": peer}, device_id_type=MESH)
+    beside.start()
+    loads, at = [], 0
+    for i, w in enumerate(weights):
+        loads.append(pltpu.make_async_copy(w, wbuf.at[:, pl.ds(at, w.shape[1])], ldsem.at[i]))
+        at += w.shape[1]
+    cuts = [(sum(widths[:i]), sum(widths[:i + 1])) for i in range(6)]
+    for c in loads:
+        c.start()
+    for c in loads:
+        c.wait()
+    beside.wait_recv()
+
+    def weight(t):
+        return wbuf[pl.ds(pl.multiple_of(t * feats, feats), feats), :]
+
+    def near(c, carry):
+        part = pl.ds(pl.multiple_of(c * step_rows, step_rows), step_rows)
+        pacc[part, :] = dot(x[part, :], weight(tp)) + dot(seg[peer, part, :], weight(peer))
+        return carry
+
+    lax.fori_loop(0, steps, near, 0)
+
+    def far(c, carry):
+        part = pl.ds(pl.multiple_of(c * step_rows, step_rows), step_rows)
+        total = pacc[part, :]
+        for d in range(xs - 1):
+            source = (xi + xs - d - 1) % xs
+            across(c, d).wait_recv()
+            relay(c, d).start()
+            total += dot(seg[source * 2 + core, part, :], weight(source * 2 + core))
+            relay(c, d).wait_recv()
+            total += dot(seg[source * 2 + 1 - core, part, :], weight(source * 2 + 1 - core))
+        pieces = [total[:, a:b] for a, b in cuts]
+        dk[part, :] = pieces[4].astype(BF16)
+        dvT[:, part] = pieces[5].T.astype(BF16)
+        wqT[:, part] = (pieces[0] * (HEAD ** -0.5 * LOG2E)).T.astype(BF16)
+        wk[part, :] = pieces[1].astype(BF16)
+        wvT[:, part] = pieces[2].T.astype(BF16)
+        dqT[:, part] = (pieces[3] * (DQK ** -0.5 * LOG2E)).T.astype(BF16)
+        for d in (0, 1):
+            first(0, d, c).start()
+            first(1, d, c).start()
+        return carry
+
+    lax.fori_loop(0, steps, far, 0)
+
     halos = []
     for i, (src, dst, to) in enumerate((
         (wk.at[pl.ds(rows - W, W)], kwin.at[pl.ds(0, W)], nxt),
@@ -69,25 +174,6 @@
             device_id={"sp": to}, device_id_type=MESH)
         c.start()
         halos.append(c)
-
-    def kcopy(direction, s, first=False):
-        slot = (me + n - s) % n if direction == 0 else (me + s) % n
-        return pltpu.make_async_remote_copy(
-            src_ref=dk if first else kbuf.at[slot], dst_ref=kbuf.at[slot],
-            send_sem=ksem.at[0, direction, s], recv_sem=ksem.at[1, direction, s],
-            device_id={"sp": right if direction == 0 else left}, device_id_type=MESH)
-
-    def vcopy(direction, s, first=False):
-        slot = (me + n - s) % n if direction == 0 else (me + s) % n
-        return pltpu.make_async_remote_copy(
-            src_ref=dvT if first else vbuf.at[slot], dst_ref=vbuf.at[slot],
-            send_sem=vsem.at[0, direction, s], recv_sem=vsem.at[1, direction, s],
-            device_id={"sp": right if direction == 0 else left}, device_id_type=MESH)
-
-    for d in (0, 1):
-        kcopy(d, 0, True).start()
-        vcopy(d, 0, True).start()
-
     cut = wo.shape[0]
     shared = [
         pltpu.make_async_remote_copy(
@@ -97,11 +183,12 @@
     ]
     for c in shared:
         c.start()
-
     local = [
         pltpu.make_async_copy(wk, kwin.at[pl.ds(W, rows)], lsem.at[0]),
         pltpu.make_async_copy(wvT, vwin.at[:, pl.ds(W, rows)], lsem.at[1]),
     ]
+    for c in local:
+        c.start()
     live = length[0]
     offset = sp * rows
     rowid = lax.broadcasted_iota(jnp.int32, (128, rows), 0) // DQK
@@ -141,9 +228,24 @@
         lax.fori_loop(0, heads, head, 0)
 
     block(dk, dvT, me)
-    for c in local[:2]:
-        c.start()
-    for c in local[:2]:
+
+    def relay_near(s):
+        arrived(0, 0, s)
+        hop(0, 0, s + 1).start()
+        arrived(1, 1, s)
+        hop(1, 1, s + 1).start()
+
+    def relay_rest(s):
+        arrived(1, 0, s)
+        arrived(0, 1, s)
+
+        @pl.when(s < half - 2)
+        def _():
+            hop(1, 0, s + 1).start()
+            hop(0, 1, s + 1).start()
+
+    relay_near(0)
+    for c in local:
         c.wait()
     for c in halos:
         c.wait()
@@ -188,22 +290,22 @@
                 out[(j * GROUP + g) * HEAD:(j * GROUP + g + 1) * HEAD, pl.ds(at, W)] = piece
         return carry
 
-    lax.fori_loop(0, rows // W, qblock, 0)
 
     def step(s, carry):
-        kcopy(0, s).wait_recv()
-        kcopy(0, s + 1).start()
-        vcopy(1, s).wait_recv()
-        vcopy(1, s + 1).start()
-        vcopy(0, s).wait_recv()
-        kcopy(1, s).wait_recv()
-
-        @pl.when(s < half - 2)
+        relay_rest(s)
+
+        @pl.when(s == 0)
         def _():
-            vcopy(0, s + 1).start()
-            kcopy(1, s + 1).start()
+            lax.fori_loop(0, rows // W, qblock, 0)
 
         def side(i, c):
+            @pl.when((i == 1) & (s < half - 2))
+            def _():
+                hop(0, 0, s + 1).wait_recv()
+                hop(0, 0, s + 2).start()
+                hop(1, 1, s + 1).wait_recv()
+                hop(1, 1, s + 2).start()
+
             origin = (me + n + (2 * i - 1) * (s + 1)) % n
             block(kbuf.at[origin], vbuf.at[origin], origin)
             return c
@@ -212,10 +314,10 @@
         return carry
 
     lax.fori_loop(0, half - 1, step, 0)
-    kcopy(0, half - 1).wait_recv()
-    vcopy(1, half - 1).wait_recv()
-    far = (me + half) % n
-    block(kbuf.at[far], vbuf.at[far], far)
+    hop(0, 0, half - 1).wait_recv()
+    hop(1, 1, half - 1).wait_recv()
+    distant = (me + half) % n
+    block(kbuf.at[distant], vbuf.at[distant], distant)
 
     qlive = offset + lax.broadcasted_iota(jnp.int32, (1, rows), 1) < live
     base = wqT.shape[0]
@@ -234,38 +336,65 @@
         w = min(128, hidden - c0)
         out_rows[:, c0:c0 + w] = out[c0:c0 + w, :].T
 
+    beside.wait_send()
+    for c in range(steps):
+        for d in range(xs - 1):
+            across(c, d).wait_send()
+            relay(c, d).wait_send()
+        for d in (0, 1):
+            first(0, d, c).wait_send()
+            first(1, d, c).wait_send()
     for d in (0, 1):
-        for s in range(half):
+        for s in range(1, half):
             if s < half - 1 or d == 0:
-                kcopy(d, s, s == 0).wait_send()
+                hop(0, d, s).wait_send()
             if s < half - 1 or d == 1:
-                vcopy(d, s, s == 0).wait_send()
+                hop(1, d, s).wait_send()
     for c in shared:
         c.wait()
 
 
-def attention(n, length, sink, lam, gain, wqT, wk, wvT, dqT, dk, dvT, wo, do):
-    hidden = wqT.shape[0] + dqT.shape[0]
-    rows = wk.shape[0]
-    heads = dqT.shape[0] // HEAD
+def layer(n, xs, length, sink, lam, gain, x, weights, wo, do):
+    rows, feats = x.shape
+    widths = [w.shape[1] for w in weights]
+    steps = rows // 128
+    depth = weights[0].shape[0]
+    if any(w % 128 for w in widths):
+        weights = [jnp.concatenate(weights, axis=1)]
+    hidden = wo.shape[0] + do.shape[0]
+    heads = widths[3] // HEAD
     half = n // 2
     return pl.pallas_call(
-        functools.partial(attention_kernel, n),
+        functools.partial(layer_kernel, n, xs, widths),
         out_shape=(
             jax.ShapeDtypeStruct((rows, hidden), BF16),
             jax.ShapeDtypeStruct((hidden, wo.shape[1]), BF16),
         ),
-        in_specs=[SM, SM, SM] + [VM] * 7 + [ANY] * 2,
+        in_specs=[SM, SM, SM, VM, VM] + [ANY] * (len(weights) + 2),
         out_specs=(VM, ANY),
         scratch_shapes=[
+            pltpu.VMEM((widths[0], rows), BF16),
+            pltpu.VMEM((rows, widths[1]), BF16),
+            pltpu.VMEM((widths[2], rows), BF16),
+            pltpu.VMEM((widths[3], rows), BF16),
+            pltpu.VMEM((rows, widths[4]), BF16),
+            pltpu.VMEM((widths[5], rows), BF16),
+            pltpu.VMEM((2 * xs, rows, feats), BF16),
+            pltpu.VMEM((depth, sum(widths)), BF16),
+            pltpu.VMEM((rows, sum(widths)), F32),
             pltpu.VMEM((hidden, rows), BF16),
-            pltpu.VMEM((n,) + dk.shape, BF16),
-            pltpu.VMEM((n,) + dvT.shape, BF16),
-            pltpu.VMEM((rows + 2 * WINDOW, wk.shape[1]), BF16),
-            pltpu.VMEM((wvT.shape[0], rows + 2 * WINDOW), BF16),
+            pltpu.VMEM((n, rows, widths[4]), BF16),
+            pltpu.VMEM((n, widths[5], rows), BF16),
+            pltpu.VMEM((rows + 2 * WINDOW, widths[1]), BF16),
+            pltpu.VMEM((widths[2], rows + 2 * WINDOW), BF16),
             pltpu.VMEM((heads, 2, 128, rows), BF16),
             pltpu.VMEM((heads, 2, HEAD + 16, rows), F32),
             pltpu.VMEM((heads, 2, 1, rows), F32),
+            pltpu.SemaphoreType.DMA((6,)),
+            pltpu.SemaphoreType.DMA((2,)),
+            pltpu.SemaphoreType.DMA((2, xs - 1, steps)),
+            pltpu.SemaphoreType.DMA((2, xs - 1, steps)),
+            pltpu.SemaphoreType.DMA((2, 2, 2, steps)),
             pltpu.SemaphoreType.DMA((2, 2, half)),
             pltpu.SemaphoreType.DMA((2, 2, half)),
             pltpu.SemaphoreType.DMA((2, 4)),
@@ -274,123 +403,8 @@
         ],
         compiler_params=pltpu.CompilerParams(
             collective_id=1, has_side_effects=True, vmem_limit_bytes=60 * 1024 * 1024),
-        name="attention",
-    )(length, sink, lam, gain, wqT, wk, wvT, dqT, dk, dvT, wo, do)
-
-
-def gather_kernel(
-    xs, widths, x, *refs,
-):
-    weights = refs[:-13]
-    wqT, wk, wvT, dqT, dk, dvT, seg, wbuf, acc, wsem, psem, xsem, rsem = refs[-13:]
-    rows, feats = x.shape
-    step_rows = 128
-    steps = rows // step_rows
-    tp = lax.axis_index("tp")
-    core = tp % 2
-    xi = tp // 2
-    peer = xi * 2 + 1 - core
-    others = [((xi + d) % xs) * 2 + core for d in range(1, xs)]
-    barrier = pltpu.get_barrier_semaphore()
-    for d in others + [peer]:
-        pl.semaphore_signal(barrier, inc=1, device_id={"tp": d}, device_id_type=MESH)
-    pl.semaphore_wait(barrier, xs)
-
-    def across(c, d):
-        part = pl.ds(pl.multiple_of(c * step_rows, step_rows), step_rows)
-        return pltpu.make_async_remote_copy(
-            src_ref=x.at[part], dst_ref=seg.at[tp, part], send_sem=xsem.at[0, d, c],
-            recv_sem=xsem.at[1, d, c], device_id={"tp": others[d]}, device_id_type=MESH)
-
-    def relay(c, d):
-        source = ((xi + xs - d - 1) % xs) * 2 + core
-        part = pl.ds(pl.multiple_of(c * step_rows, step_rows), step_rows)
-        return pltpu.make_async_remote_copy(
-            src_ref=seg.at[source, part], dst_ref=seg.at[source, part], send_sem=rsem.at[0, d, c],
-            recv_sem=rsem.at[1, d, c], device_id={"tp": peer}, device_id_type=MESH)
-
-    for c in range(steps):
-        for d in range(xs - 1):
-            across(c, d).start()
-    beside = pltpu.make_async_remote_copy(
-        src_ref=x, dst_ref=seg.at[tp], send_sem=psem.at[0], recv_sem=psem.at[1],
-        device_id={"tp": peer}, device_id_type=MESH)
-    beside.start()
-    loads, at = [], 0
-    for i, w in enumerate(weights):
-        loads.append(pltpu.make_async_copy(w, wbuf.at[:, pl.ds(at, w.shape[1])], wsem.at[i]))
-        at += w.shape[1]
-    cuts = [(sum(widths[:i]), sum(widths[:i + 1])) for i in range(6)]
-    for c in loads:
-        c.start()
-    for c in loads:
-        c.wait()
-    beside.wait_recv()
-
-    def weight(t):
-        return wbuf[pl.ds(pl.multiple_of(t * feats, feats), feats), :]
-
-    def near(c, carry):
-        part = pl.ds(pl.multiple_of(c * step_rows, step_rows), step_rows)
-        acc[part, :] = dot(x[part, :], weight(tp)) + dot(seg[peer, part, :], weight(peer))
-        return carry
-
-    lax.fori_loop(0, steps, near, 0)
-
-    def far(c, carry):
-        part = pl.ds(pl.multiple_of(c * step_rows, step_rows), step_rows)
-        total = acc[part, :]
-        for d in range(xs - 1):
-            source = (xi + xs - d - 1) % xs
-            across(c, d).wait_recv()
-            relay(c, d).start()
-            total += dot(seg[source * 2 + core, part, :], weight(source * 2 + core))
-            relay(c, d).wait_recv()
-            total += dot(seg[source * 2 + 1 - core, part, :], weight(source * 2 + 1 - core))
-        pieces = [total[:, a:b] for a, b in cuts]
-        wqT[:, part] = (pieces[0] * (HEAD ** -0.5 * LOG2E)).T.astype(BF16)
-        wk[part, :] = pieces[1].astype(BF16)
-        wvT[:, part] = pieces[2].T.astype(BF16)
-        dqT[:, part] = (pieces[3] * (DQK ** -0.5 * LOG2E)).T.astype(BF16)
-        dk[part, :] = pieces[4].astype(BF16)
-        dvT[:, part] = pieces[5].T.astype(BF16)
-        return carry
-
-    lax.fori_loop(0, steps, far, 0)
-    beside.wait_send()
-    for c in range(steps):
-        for d in range(xs - 1):
-            across(c, d).wait_send()
-            relay(c, d).wait_send()
-
-
-def gather(xs, x, *weights):
-    rows, feats = x.shape
-    widths = [w.shape[1] for w in weights]
-    steps = rows // 128
-    depth = weights[0].shape[0]
-    if any(w % 128 for w in widths):
-        weights = [jnp.concatenate(weights, axis=1)]
-    shapes = [(widths[0], rows), (rows, widths[1]), (widths[2], rows),
-              (widths[3], rows), (rows, widths[4]), (widths[5], rows)]
-    return pl.pallas_call(
-        functools.partial(gather_kernel, xs, widths),
-        out_shape=[jax.ShapeDtypeStruct(s, BF16) for s in shapes],
-        in_specs=[VM] + [ANY] * len(weights),
-        out_specs=[VM] * 6,
-        scratch_shapes=[
-            pltpu.VMEM((2 * xs, rows, feats), BF16),
-            pltpu.VMEM((depth, sum(widths)), BF16),
-            pltpu.VMEM((rows, sum(widths)), F32),
-            pltpu.SemaphoreType.DMA((6,)),
-            pltpu.SemaphoreType.DMA((2,)),
-            pltpu.SemaphoreType.DMA((2, xs - 1, steps)),
-            pltpu.SemaphoreType.DMA((2, xs - 1, steps)),
-        ],
-        compiler_params=pltpu.CompilerParams(
-            collective_id=2, has_side_effects=True, vmem_limit_bytes=60 * 1024 * 1024),
-        name="gather",
-    )(x, *weights)
+        name="layer",
+    )(length, sink, lam, gain, x, *weights, wo, do)
 
 
 def project_kernel(xs, parts, a, wo, do, wp, out, wbuf, ap, sbuf, rbuf, wsem, asem, ssem):
@@ -496,10 +510,9 @@
 
 def body(n, xs, inputs, length, win_query, win_key, win_value, sink_logit, diff_query, diff_key,
          diff_value, mix_lambda, head_gain, win_out, diff_out):
-    wqT, wk, wvT, dqT, dk, dvT = gather(
-        xs, inputs, win_query, win_key, win_value, diff_query, diff_key, diff_value)
-    rows, wp = attention(n, length, sink_logit, mix_lambda, head_gain.reshape(-1, 1),
-                         wqT, wk, wvT, dqT, dk, dvT, win_out, diff_out)
+    weights = [win_query, win_key, win_value, diff_query, diff_key, diff_value]
+    rows, wp = layer(n, xs, length, sink_logit, mix_lambda, head_gain.reshape(-1, 1), inputs,
+                     weights, win_out, diff_out)
     return project(xs, rows, win_out, diff_out, wp)
 
 

time: 134 us -> 127 us (0.948)
  Pallas kernels: 130 us -> 122 us
    pallas_call x2 -> x1, Pallas kernels: 99.6 us -> 91.7 us  [layer(): pl.pallas_call(functools.partial(layer_kernel, n, xs, widths), out_shape=...]
where the time goes in v3:
time: 127 us
  Pallas kernels  122 us (96%)
  local copies, waits for them, and re-layouts  3.65 us (3%)
    pallas_call x1, Pallas kernels, layer(): pl.pallas_call(functools.partial(layer_kernel, n, xs, widths), out_shape=...  91.7 us
    pallas_call x1, Pallas kernels, project(): pl.pallas_call(functools.partial(project_kernel, xs, parts), out_shape=ja...  30.5 us

profile of v3, /device:TPU:0, one launch (start us, length us, event | category | flops | bytes accessed | tf_op | source)
XLA Modules:
  0.0 126.6 jit_solution(1099586436301411954)
XLA Ops:
  0.7 1.4 %copy.14.gain = f32[64,1]{1,0:T(8,128)} copy(f32[64,1]{0,1:T(1,128)} %bitcast.1) | data formatting | bytes 512 | tf_op jit(solution)/shard_map/reshape | solution.py:514
  2.0 91.7 %layer.1 = (bf16[512,640]{1,0:T(8,128)(2,1)}, bf16[640,4096]{1,0:T(8,128)(2,1)}) custom-call(s32[1]{0:T(128)S(6)} %copy.16.length, f32[6]{0:T(128)} %sink.1, f32[4]{0:T(128)} %lam.1, f32[64,1]{1,0:T(8,128)} %copy.14.gain, bf16[512,1024]{1,0:T(8,128)(2,1)} %x.1, bf16[4096,384]{1,0:T(8,128)(2,1)} %refs_0_.1, bf16[4096,128]{1,0:T(8,128)(2,1)} %refs_1_.1, ...), custom_call_target="tpu_custom_call" | custom-call | tf_op jit(solution)/shard_map/layer/pallas_call | solution.py:367
  93.7 30.5 %project.1 = bf16[128,4096]{1,0:T(8,128)(2,1)} custom-call(bf16[512,640]{1,0:T(8,128)(2,1)} %get-tuple-element.7.a, bf16[384,4096]{1,0:T(8,128)(2,1)} %wo.1, bf16[256,4096]{1,0:T(8,128)(2,1)} %do.1, bf16[640,4096]{1,0:T(8,128)(2,1)} %get-tuple-element.8.wp), custom_call_target="tpu_custom_call" | custom-call | tf_op jit(solution)/shard_map/project/pallas_call | solution.py:491
  124.3 2.3 %copy.17 = bf16[128,4096]{1,0:T(8,128)(2,1)} copy(bf16[128,4096]{1,0:T(8,128)(2,1)} %project.1) | data formatting | bytes 2097152

commit v4 on v3

--- a/solution.py
+++ b/solution.py
@@ -213,16 +213,20 @@
             kt = ksrc[:, pl.ds(pl.multiple_of((h // 2) * 128, 128), 128)]
             vt = vsrc[pl.ds(pl.multiple_of(h * HEAD, HEAD), HEAD), :] * vlive
             vx = jnp.concatenate([vt, ones], axis=0)
-            for m in (0, 1):
-                for q0 in range(0, rows, 256):
-                    cols = pl.ds(q0, 256)
-                    s = dot(kt, qz[h, m, :, cols])
-                    s = jnp.where(klive, s, NEG)
-                    old = mx[h, m, :, cols]
-                    new = jnp.maximum(old, jnp.max(s, axis=0, keepdims=True))
-                    p = jnp.exp2(s - new).astype(BF16)
-                    acc[h, m, :, cols] = acc[h, m, :, cols] * jnp.exp2(old - new) + dot(vx, p)
-                    mx[h, m, :, cols] = new
+            tiles = [(m, q0) for m in (0, 1) for q0 in range(0, rows, 512)]
+            nexts = dot(kt, qz[h, 0, :, pl.ds(0, 512)])
+            for i, (m, q0) in enumerate(tiles):
+                s = nexts
+                if i + 1 < len(tiles):
+                    m1, q1 = tiles[i + 1]
+                    nexts = dot(kt, qz[h, m1, :, pl.ds(q1, 512)])
+                cols = pl.ds(q0, 512)
+                s = jnp.where(klive, s, NEG)
+                old = mx[h, m, :, cols]
+                new = jnp.maximum(old, jnp.max(s, axis=0, keepdims=True))
+                p = jnp.exp2(s - new).astype(BF16)
+                acc[h, m, :, cols] = acc[h, m, :, cols] * jnp.exp2(old - new) + dot(vx, p)
+                mx[h, m, :, cols] = new
             return carry
 
         lax.fori_loop(0, heads, head, 0)
@@ -321,6 +325,7 @@
 
     qlive = offset + lax.broadcasted_iota(jnp.int32, (1, rows), 1) < live
     base = wqT.shape[0]
+    column = jnp.broadcast_to(gain[...], (128, HEAD)).T[:, 0:1]
     for h in range(heads):
         a0 = acc[h, 0]
         a1 = acc[h, 1]
@@ -328,7 +333,7 @@
         t1 = a1[HEAD:HEAD + 1]
         mixed = a0[:HEAD] / t0 - lam[h] * (a1[:HEAD] / t1)
         ms = jnp.mean(mixed * mixed, axis=0, keepdims=True)
-        r = mixed * lax.rsqrt(ms + EPS) * gain[...]
+        r = mixed * lax.rsqrt(ms + EPS) * column
         out[base + h * HEAD:base + (h + 1) * HEAD, :] = jnp.where(qlive, r, 0.0).astype(BF16)
 
     hidden = out.shape[0]
@@ -511,7 +516,7 @@
 def body(n, xs, inputs, length, win_query, win_key, win_value, sink_logit, diff_query, diff_key,
          diff_value, mix_lambda, head_gain, win_out, diff_out):
     weights = [win_query, win_key, win_value, diff_query, diff_key, diff_value]
-    rows, wp = layer(n, xs, length, sink_logit, mix_lambda, head_gain.reshape(-1, 1), inputs,
+    rows, wp = layer(n, xs, length, sink_logit, mix_lambda, head_gain.reshape(1, -1), inputs,
                      weights, win_out, diff_out)
     return project(xs, rows, win_out, diff_out, wp)
 

time: 127 us -> 108 us (0.85)
  Pallas kernels: 122 us -> 105 us
  local copies, waits for them, and re-layouts: 3.65 us -> 2.29 us
    pallas_call x1, Pallas kernels: 91.7 us -> 74.6 us  [layer(): pl.pallas_call(functools.partial(layer_kernel, n, xs, widths), out_shape=...]
    reshape x1 -> x0, local copies, waits for them, and re-layouts: 1.36 us -> none  [body(): head_gain.reshape(-1, 1)]
where the time goes in v4:
time: 108 us
  Pallas kernels  105 us (97%)
  local copies, waits for them, and re-layouts  2.29 us (2%)
    pallas_call x1, Pallas kernels, layer(): pl.pallas_call(functools.partial(layer_kernel, n, xs, widths), out_shape=...  74.6 us
    pallas_call x1, Pallas kernels, project(): pl.pallas_call(functools.partial(project_kernel, xs, parts), out_shape=ja...  30.2 us
    unnamed x1, local copies, waits for them, and re-layouts  2.29 us

profile of v4, /device:TPU:0, one launch (start us, length us, event | category | flops | bytes accessed | tf_op | source)
XLA Modules:
  0.0 107.8 jit_solution(3701910036935694669)
XLA Ops:
  0.7 74.6 %layer.1 = (bf16[512,640]{1,0:T(8,128)(2,1)}, bf16[640,4096]{1,0:T(8,128)(2,1)}) custom-call(s32[1]{0:T(128)S(6)} %copy.15.length, f32[6]{0:T(128)} %sink.1, f32[4]{0:T(128)} %lam.1, f32[1,64]{1,0:T(1,128)} %bitcast.1, bf16[512,1024]{1,0:T(8,128)(2,1)} %x.1, bf16[4096,384]{1,0:T(8,128)(2,1)} %refs_0_.1, bf16[4096,128]{1,0:T(8,128)(2,1)} %refs_1_.1, ...), custom_call_target="tpu_custom_call" | custom-call | tf_op jit(solution)/shard_map/layer/pallas_call | solution.py:372
  75.3 30.2 %project.1 = bf16[128,4096]{1,0:T(8,128)(2,1)} custom-call(bf16[512,640]{1,0:T(8,128)(2,1)} %get-tuple-element.7.a, bf16[384,4096]{1,0:T(8,128)(2,1)} %wo.1, bf16[256,4096]{1,0:T(8,128)(2,1)} %do.1, bf16[640,4096]{1,0:T(8,128)(2,1)} %get-tuple-element.8.wp), custom_call_target="tpu_custom_call" | custom-call | tf_op jit(solution)/shard_map/project/pallas_call | solution.py:496
  105.5 2.3 %copy.16 = bf16[128,4096]{1,0:T(8,128)(2,1)} copy(bf16[128,4096]{1,0:T(8,128)(2,1)} %project.1) | data formatting | bytes 2097152
